TPU v7x, 32 devices: a whole 2x2x4 slice. The times are simulated.
32 devices in a mesh: grp: 2 (over y), sp: 4 (over z), tp: 4 (over x, core).
Axes of the slice: x: 2, y: 2, z: 4, core: 2. Of those that a mesh axis runs over, the one named last changes fastest.
Arguments:
- latent: bfloat16 [4096, 4096], P(('grp', 'sp', 'tp')), parts along dimension 0, may hold values from -260 to 260
- context: bfloat16 [1536, 4096], P(('grp', 'sp')), parts along dimension 0, may hold values from -6 to 6
- conditioning: bfloat16 [8192], P(('grp', 'sp')), parts along dimension 0, may hold values from -6 to 6
- norm_gain: float32 [4096], replicated, may hold values from 0.1 to 1.9
- shift_weight: bfloat16 [4096, 4096], P('sp', 'tp'), may hold values from -0.09375 to 0.09375
- scale_weight: bfloat16 [4096, 4096], P('sp', 'tp'), may hold values from -0.09375 to 0.09375
- gate_weight: bfloat16 [4096, 4096], P('sp', 'tp'), may hold values from -0.09375 to 0.09375
- query_weight: bfloat16 [4096, 1024], P(None, 'tp'), may hold values from -3 to 3
- key_weight: bfloat16 [4096, 512], P(None, 'tp'), may hold values from -3 to 3
- value_weight: bfloat16 [4096, 512], P(None, 'tp'), may hold values from -0.09375 to 0.09375
- out_weight: bfloat16 [1024, 4096], P(None, 'tp'), may hold values from -1.5 to 1.5
- sink_logit: float32 [16], P('tp'), may hold values from 3 to 7
Outputs:
- mixed: bfloat16 [4096, 4096], P(('grp', 'sp', 'tp')), parts along dimension 0
There are 2 independent parts, one for each index of `grp`. A program takes and returns all parts, laid end to end along the dimension named above; an argument that names none is the same for every part. Nothing has to cross between parts.
All inputs are finite; a program needn't handle non-finite values.
Results may differ from a plain program's by a relative error of at most 0.012.
The roundings to bfloat16 on the way count: a program that leaves them out, or rounds other values in their place, can miss the bound.
Values may be sent and summed in bfloat16 or wider, within the bound.
A program may use at most 64 MiB of HBM per device.

v0:
```python
import functools

import jax
import jax.numpy as jnp
from jax import lax
from jax.experimental import pallas as pl
from jax.experimental.pallas import tpu as pltpu
from jax.sharding import PartitionSpec as P

HEADS = 16
KV_HEADS = 8
HD = 64
GRID_W = 64
WIN = 128


epsilon = 1e-06
rope_base = 10000.0
neg_large = -1e30


def with_halo(cells, sides, width):
    for axis, dim in sides:
        count = lax.axis_size(axis)
        ends = count - 1
        head = lax.slice_in_dim(cells, 0, width, axis=dim)
        tail = lax.slice_in_dim(cells, cells.shape[dim] - width, cells.shape[dim], axis=dim)
        cells = jnp.concatenate(
            [
                lax.ppermute(tail, axis, [(i, (i + 1) % count) for i in range(ends)]),
                cells,
                lax.ppermute(head, axis, [((i + 1) % count, i) for i in range(ends)]),
            ],
            axis=dim,
        )
    return cells


def row_norm(matrix, norm_gain):
    values = matrix.astype(jnp.float32)
    return (
        values * lax.rsqrt(jnp.mean(values * values, axis=-1, keepdims=True) + epsilon) * norm_gain
    )


def axial_turn(values, position):
    half_dim = values.shape[-1] // 2
    quarter = half_dim // 2
    inverse = rope_base ** (-jnp.arange(quarter, dtype=jnp.float32) / quarter)

    def turn(section, coordinate):
        angles = coordinate.astype(jnp.float32)[:, None] * inverse[None, :]
        cosine = jnp.cos(angles)[:, None, :]
        sine_part = jnp.sin(angles)[:, None, :]
        leading = section[..., :quarter]
        trailing = section[..., quarter:]
        return jnp.concatenate(
            [leading * cosine - trailing * sine_part, leading * sine_part + trailing * cosine],
            axis=-1,
        )

    return jnp.concatenate(
        [
            turn(values[..., :half_dim], position // GRID_W),
            turn(values[..., half_dim:], position % GRID_W),
        ],
        axis=-1,
    )


def context_pairs(context_rows, norm_gain, key_weight, value_weight):
    prepared = row_norm(context_rows, norm_gain).astype(jnp.bfloat16)
    return jnp.concatenate(
        [
            jnp.dot(prepared, key_weight, preferred_element_type=jnp.float32),
            jnp.dot(prepared, value_weight, preferred_element_type=jnp.float32),
        ],
        axis=1,
    ).astype(jnp.bfloat16)


def local_plain(
    latent,
    context,
    conditioning,
    norm_gain,
    shift_weight,
    scale_weight,
    gate_weight,
    query_weight,
    key_weight,
    value_weight,
    out_weight,
    sink_logit,
):
    lifted = jax.nn.silu(conditioning.astype(jnp.float32)).astype(jnp.bfloat16)[None, :]
    shift_part = jnp.dot(lifted, shift_weight, preferred_element_type=jnp.float32)[0]
    scale_part = jnp.dot(lifted, scale_weight, preferred_element_type=jnp.float32)[0]
    gate_part = jnp.dot(lifted, gate_weight, preferred_element_type=jnp.float32)[0]
    summed = lax.psum((shift_part, scale_part, gate_part), "sp")
    shift_vec, scale_vec, gate_vec = (
        lax.all_gather(summed[0], "tp", axis=0, tiled=True),
        lax.all_gather(summed[1], "tp", axis=0, tiled=True),
        lax.all_gather(summed[2], "tp", axis=0, tiled=True),
    )
    normed = (row_norm(latent, norm_gain) * (1.0 + scale_vec) + shift_vec).astype(jnp.bfloat16)
    segment = lax.all_gather(normed, "tp", axis=0, tiled=True)
    projected = jnp.concatenate(
        [
            jnp.dot(segment, query_weight, preferred_element_type=jnp.float32),
            jnp.dot(segment, key_weight, preferred_element_type=jnp.float32),
            jnp.dot(segment, value_weight, preferred_element_type=jnp.float32),
        ],
        axis=1,
    )
    row_count = projected.shape[0]
    query_width = query_weight.shape[1]
    key_width = key_weight.shape[1]
    query_heads = query_width // HD
    pair_heads = key_width // HD
    group_size = HEADS // KV_HEADS
    row_offset = lax.axis_index("sp") * row_count
    position = row_offset + jnp.arange(row_count, dtype=jnp.int32)
    queries = axial_turn(
        projected[:, :query_width].reshape(row_count, query_heads, HD), position
    ).astype(jnp.bfloat16)
    latent_keys = axial_turn(
        projected[:, query_width : query_width + key_width].reshape(row_count, pair_heads, HD),
        position,
    ).astype(jnp.bfloat16)
    latent_values = projected[:, query_width + key_width :].astype(jnp.bfloat16)
    key_value = jnp.concatenate([latent_keys.reshape(row_count, key_width), latent_values], axis=1)
    widened = with_halo(key_value, (("sp", 0),), WIN)
    context_all = lax.all_gather(
        context_pairs(context, norm_gain, key_weight, value_weight), "sp", axis=0, tiled=True
    )
    block_count = row_count // WIN
    context_count = context_all.shape[0]
    query_blocks = queries.reshape(block_count, WIN, pair_heads, group_size, HD)
    band_blocks = widened.reshape(block_count + 2, WIN, 2 * key_width)
    band_rows = jnp.concatenate(
        [band_blocks[:block_count], band_blocks[1 : block_count + 1], band_blocks[2:]], axis=1
    )
    band_keys = band_rows[..., :key_width].reshape(block_count, 3 * WIN, pair_heads, HD)
    band_values = band_rows[..., key_width:].reshape(block_count, 3 * WIN, pair_heads, HD)
    context_keys = context_all[:, :key_width].reshape(context_count, pair_heads, HD)
    context_values = context_all[:, key_width:].reshape(context_count, pair_heads, HD)
    factor = HD ** (-0.5)
    local_scores = (
        jnp.einsum("nqhgd,nkhd->nhgqk", query_blocks, band_keys, preferred_element_type=jnp.float32)
        * factor
    )
    query_pos = position.reshape(block_count, WIN)
    key_pos = (
        row_offset
        - WIN
        + jnp.arange(block_count, dtype=jnp.int32)[:, None] * WIN
        + jnp.arange(3 * WIN, dtype=jnp.int32)[None, :]
    )
    seq_total = row_count * lax.axis_size("sp")
    allowed = (
        (jnp.abs(key_pos[:, None, :] - query_pos[:, :, None]) <= WIN)
        & (key_pos[:, None, :] >= 0)
        & (key_pos[:, None, :] < seq_total)
    )
    local_scores = jnp.where(allowed[:, None, None], local_scores, neg_large)
    context_scores = (
        jnp.einsum(
            "nqhgd,thd->nhgqt", query_blocks, context_keys, preferred_element_type=jnp.float32
        )
        * factor
    )
    sink_values = sink_logit.reshape(pair_heads, group_size)[None, :, :, None, None]
    highest = jnp.maximum(
        jnp.maximum(
            jnp.max(local_scores, axis=-1, keepdims=True),
            jnp.max(context_scores, axis=-1, keepdims=True),
        ),
        sink_values,
    )
    local_exp = jnp.exp(local_scores - highest)
    context_exp = jnp.exp(context_scores - highest)
    denominator = (
        jnp.sum(local_exp, axis=-1, keepdims=True)
        + jnp.sum(context_exp, axis=-1, keepdims=True)
        + jnp.exp(sink_values - highest)
    )
    local_weights = (local_exp / denominator).astype(jnp.bfloat16)
    context_weights = (context_exp / denominator).astype(jnp.bfloat16)
    attended = jnp.einsum(
        "nhgqk,nkhd->nqhgd", local_weights, band_values, preferred_element_type=jnp.float32
    ) + jnp.einsum(
        "nhgqt,thd->nqhgd", context_weights, context_values, preferred_element_type=jnp.float32
    )
    attended = attended.reshape(row_count, query_width).astype(jnp.bfloat16)
    columns_part = jnp.dot(
        lax.all_gather(attended, "tp", axis=1, tiled=True),
        out_weight,
        preferred_element_type=jnp.float32,
    ).astype(jnp.bfloat16)
    blended = lax.all_to_all(columns_part, "tp", split_axis=0, concat_axis=1, tiled=True)
    return (latent.astype(jnp.float32) + gate_vec * blended.astype(jnp.float32)).astype(
        jnp.bfloat16
    )


PIECES = 4
NORM_ROWS = 16


def remote(src, dst, send, recv, axis, peer):
    return pltpu.make_async_remote_copy(
        src_ref=src,
        dst_ref=dst,
        send_sem=send,
        recv_sem=recv,
        device_id={axis: peer},
        device_id_type=pl.DeviceIdType.MESH,
    )


def fused_kernel(
    tp,
    sp,
    latent,
    context,
    conditioning,
    norm_gain,
    shift_weight,
    scale_weight,
    gate_weight,
    query_weight,
    key_weight,
    value_weight,
    out_weight,
    sink,
    blended,
    gate_out,
    cond_v,
    gain_v,
    mod_w,
    wq,
    wk,
    wv,
    wo,
    ctx_v,
    rows_all,
    normed,
    mod_part,
    mod_all,
    factor_v,
    shift_v,
    gate_v,
    turn_cos,
    turn_sin,
    queries,
    key_value,
    ctx_kv,
    att_all,
    out_cols,
    load_sem,
    pair_send,
    pair_recv,
    far_send,
    far_recv,
    fwd_send,
    fwd_recv,
    modsp_send,
    modsp_recv,
    modtp_send,
    modtp_recv,
    ctx_send,
    ctx_recv,
    halo_send,
    halo_recv,
    apair_send,
    apair_recv,
    afar_send,
    afar_recv,
    afwd_send,
    afwd_recv,
    out_send,
    out_recv,
):
    t = lax.axis_index("tp")
    s = lax.axis_index("sp")
    chips = tp // 2
    core = lax.rem(t, 2)
    chip = t // 2
    pair = chip * 2 + (1 - core)
    rows, width = latent.shape
    ctx_rows = context.shape[0]
    mod_cols = shift_weight.shape[1]
    query_width = query_weight.shape[1]
    key_width = key_weight.shape[1]
    heads = query_width // HD
    group = heads // (key_width // HD)
    total = tp * rows
    out_width = out_weight.shape[1]
    piece = rows // PIECES
    f32, bf16 = jnp.float32, jnp.bfloat16

    def chip_at(j):
        return lax.rem(chip + j, chips)

    def chip_from(j):
        return lax.rem(chip + chips - j, chips)

    loads = [
        (conditioning, cond_v),
        (shift_weight, mod_w.at[0]),
        (scale_weight, mod_w.at[1]),
        (gate_weight, mod_w.at[2]),
        (norm_gain, gain_v),
        (context, ctx_v),
        (key_weight, wk),
        (value_weight, wv),
        (latent, rows_all.at[t]),
        (query_weight, wq),
        (out_weight, wo),
    ]
    loads = [pltpu.make_async_copy(a, b, load_sem.at[i]) for i, (a, b) in enumerate(loads)]
    for load in loads:
        load.start()

    barrier = pltpu.get_barrier_semaphore()
    for k in range(1, tp):
        pl.semaphore_signal(
            barrier, inc=1, device_id={"tp": lax.rem(t + k, tp)}, device_id_type=pl.DeviceIdType.MESH
        )
    for k in range(1, sp):
        pl.semaphore_signal(
            barrier, inc=1, device_id={"sp": lax.rem(s + k, sp)}, device_id_type=pl.DeviceIdType.MESH
        )
    pl.semaphore_wait(barrier, tp - 1 + sp - 1)

    far = {}
    for c in range(PIECES):
        part = pl.ds(c * piece, piece)
        for j in range(1, chips):
            i = (j - 1) * PIECES + c
            far[j, c] = remote(
                latent.at[part],
                rows_all.at[t, part],
                far_send.at[i],
                far_recv.at[i],
                "tp",
                chip_at(j) * 2 + core,
            )
            far[j, c].start()
    near = remote(latent, rows_all.at[t], pair_send.at[0], pair_recv.at[0], "tp", pair)
    near.start()

    for i in range(4):
        loads[i].wait()
    cond = cond_v[...].astype(f32).reshape(1, cond_v.shape[0])
    lifted = jnp.broadcast_to(cond / (1.0 + jnp.exp(-cond)), (16, cond.shape[1])).astype(bf16)
    for i in range(3):
        mod_part[s, :, i * mod_cols : (i + 1) * mod_cols] = jnp.dot(
            lifted, mod_w[i], preferred_element_type=f32
        )[0:1]
    mods = []
    for k in range(1, sp):
        copy = remote(
            mod_part.at[s],
            mod_part.at[s],
            modsp_send.at[k - 1],
            modsp_recv.at[k - 1],
            "sp",
            lax.rem(s + k, sp),
        )
        copy.start()
        mods.append(copy)

    for i in range(4, 8):
        loads[i].wait()

    def norm_context(g, carry):
        part = pl.ds(pl.multiple_of(g * NORM_ROWS, NORM_ROWS), NORM_ROWS)
        values = ctx_v[part].astype(f32)
        scale = lax.rsqrt(jnp.mean(values * values, axis=-1, keepdims=True) + epsilon)
        ctx_v[part] = (values * scale * gain_v[...]).astype(bf16)
        return carry

    lax.fori_loop(0, ctx_rows // NORM_ROWS, norm_context, 0)
    ctx_kv[s, :, :key_width] = jnp.dot(ctx_v[...], wk[...], preferred_element_type=f32).astype(bf16)
    ctx_kv[s, :, key_width:] = jnp.dot(ctx_v[...], wv[...], preferred_element_type=f32).astype(bf16)
    ctxs = []
    for k in range(1, sp):
        copy = remote(
            ctx_kv.at[s],
            ctx_kv.at[s],
            ctx_send.at[k - 1],
            ctx_recv.at[k - 1],
            "sp",
            lax.rem(s + k, sp),
        )
        copy.start()
        ctxs.append(copy)

    for copy in mods:
        copy.wait()
    summed = mod_part[0]
    for k in range(1, sp):
        summed = summed + mod_part[k]
    mod_all[t] = summed
    mods = []
    for k in range(1, tp):
        copy = remote(
            mod_all.at[t],
            mod_all.at[t],
            modtp_send.at[k - 1],
            modtp_recv.at[k - 1],
            "tp",
            lax.rem(t + k, tp),
        )
        copy.start()
        mods.append(copy)

    lane = lax.broadcasted_iota(jnp.int32, (WIN, 128), 1)
    row = lax.broadcasted_iota(jnp.int32, (WIN, 128), 0)
    quarter = HD // 4
    inverse = jnp.exp(
        lax.rem(lane, quarter).astype(f32) * (-jnp.log(jnp.float32(rope_base)) / quarter)
    )
    first = lax.rem(lane, 2 * quarter) < quarter

    def tables(b, carry):
        place = s * total + b * WIN + row
        by_row = lax.rem(lane, HD) < HD // 2
        coordinate = jnp.where(by_row, place // GRID_W, lax.rem(place, GRID_W))
        angles = coordinate.astype(f32) * inverse
        turn_cos[b] = jnp.cos(angles)
        sines = jnp.sin(angles)
        turn_sin[b] = jnp.where(first, -sines, sines)
        return carry

    lax.fori_loop(0, tp, tables, 0)

    for copy in mods:
        copy.wait()
    for i in range(tp):
        cols = slice(i * mod_cols, (i + 1) * mod_cols)
        shift_v[:, cols] = mod_all[i, :, 0:mod_cols]
        factor_v[:, cols] = gain_v[:, cols] * (1.0 + mod_all[i, :, mod_cols : 2 * mod_cols])
        gate_v[:, cols] = mod_all[i, :, 2 * mod_cols : 3 * mod_cols]
    gate_store = pltpu.make_async_copy(gate_v, gate_out, load_sem.at[len(loads)])
    gate_store.start()

    low = lane < HD

    def turned(values, slot):
        swapped = jnp.where(
            first, pltpu.roll(values, 128 - quarter, 1), pltpu.roll(values, quarter, 1)
        )
        return values * turn_cos[slot] + swapped * turn_sin[slot]

    half = rows // 2

    def norm_piece(slot, first_row, count, target):
        def norm_rows(g, carry):
            at = pl.multiple_of(first_row + g * NORM_ROWS, NORM_ROWS)
            values = rows_all[slot, pl.ds(at, NORM_ROWS)].astype(f32)
            scale = lax.rsqrt(jnp.mean(values * values, axis=-1, keepdims=True) + epsilon)
            normed[pl.ds(pl.multiple_of(target + at, NORM_ROWS), NORM_ROWS)] = (
                values * scale * factor_v[...] + shift_v[...]
            ).astype(bf16)
            return carry

        lax.fori_loop(0, count // NORM_ROWS, norm_rows, 0)

    def project(slots):
        prepared = normed[...]
        q_both = jnp.dot(prepared, wq[...], preferred_element_type=f32)
        k_both = jnp.dot(prepared, wk[...], preferred_element_type=f32)
        v_both = jnp.dot(prepared, wv[...], preferred_element_type=f32)
        factor = HD ** (-0.5)
        for i, slot in enumerate(slots):
            q, k, v = (a[i * rows : (i + 1) * rows] for a in (q_both, k_both, v_both))
            base = pl.multiple_of(WIN + slot * rows, WIN)
            key_value[pl.ds(base, rows), :key_width] = turned(k, slot).astype(bf16)
            key_value[pl.ds(base, rows), key_width:] = v.astype(bf16)
            for h in range(heads):
                lanes = q[:, (h // 2) * 128 : (h // 2 + 1) * 128]
                lanes = (turned(lanes, slot).astype(bf16).astype(f32)) * factor
                at, want = h % 2, h // group
                if at != want:
                    lanes = pltpu.roll(lanes, HD, 1)
                keep = low if want == 0 else jnp.logical_not(low)
                lanes = jnp.where(keep, lanes, 0.0).astype(bf16)
                for n in range(2):
                    queries[2 * slot + n, h * half : (h + 1) * half] = lanes[
                        n * half : (n + 1) * half
                    ]

    loads[8].wait()
    loads[9].wait()

    def fwd(j, c):
        slot = chip_from(j) * 2 + core
        part = pl.ds(c * piece, piece)
        i = (j - 1) * PIECES + c
        return remote(
            rows_all.at[slot, part],
            rows_all.at[slot, part],
            fwd_send.at[i],
            fwd_recv.at[i],
            "tp",
            pair,
        )

    norm_piece(t, 0, rows, 0)
    near.wait_recv()
    norm_piece(pair, 0, rows, rows)
    project((t, pair))
    for j in range(1, chips):
        mine, other = chip_from(j) * 2 + core, chip_from(j) * 2 + 1 - core
        for c in range(PIECES):
            far[j, c].wait_recv()
            fwd(j, c).start()
            norm_piece(mine, c * piece, piece, 0)
            if c:
                fwd(j, c - 1).wait_recv()
                norm_piece(other, (c - 1) * piece, piece, rows)
        fwd(j, PIECES - 1).wait_recv()
        norm_piece(other, (PIECES - 1) * piece, piece, rows)
        project((mine, other))

    halo_right = remote(
        key_value.at[pl.ds(total, WIN)],
        key_value.at[pl.ds(0, WIN)],
        halo_send.at[0],
        halo_recv.at[0],
        "sp",
        lax.rem(s + 1, sp),
    )
    halo_left = remote(
        key_value.at[pl.ds(WIN, WIN)],
        key_value.at[pl.ds(total + WIN, WIN)],
        halo_send.at[1],
        halo_recv.at[1],
        "sp",
        lax.rem(s + sp - 1, sp),
    )
    halo_right.start()
    halo_left.start()
    for copy in ctxs:
        copy.wait()
    loads[10].wait()

    def halves_at(p):
        inner = p < tp - 2
        return (
            jnp.where(inner, p + 2, p - (tp - 2)),
            p + tp,
        )

    def att_pair(b):
        return remote(
            att_all.at[b, t], att_all.at[b, t], apair_send.at[b], apair_recv.at[b], "tp", pair
        )

    def att_far(b, j):
        i = b * (chips - 1) + j - 1
        return remote(
            att_all.at[b, t],
            att_all.at[b, t],
            afar_send.at[i],
            afar_recv.at[i],
            "tp",
            chip_at(j) * 2 + core,
        )

    def att_fwd(b, j):
        slot = chip_from(j) * 2 + core
        i = b * (chips - 1) + j - 1
        return remote(
            att_all.at[b, slot],
            att_all.at[b, slot],
            afwd_send.at[i],
            afwd_recv.at[i],
            "tp",
            pair,
        )

    contract = (((1,), (1,)), ((), ()))
    band = 2 * WIN + half
    stack = heads * half
    q_pos = lax.rem(lax.broadcasted_iota(jnp.int32, (stack, band), 0), half)
    k_pos = lax.broadcasted_iota(jnp.int32, (stack, band), 1)
    in_window = jnp.logical_and(k_pos >= q_pos, k_pos <= q_pos + 2 * WIN)
    head_of = lax.broadcasted_iota(jnp.int32, (stack, 1), 0) // half
    sinks = jnp.full((stack, 1), sink[0], f32)
    for h in range(1, heads):
        sinks = jnp.where(head_of == h, sink[h], sinks)

    def attend(p, n, hb):
        start = pl.multiple_of(hb * half, half)
        band_k = key_value[pl.ds(start, band), :key_width]
        band_v = key_value[pl.ds(start, band), key_width:]
        ctx_k = ctx_kv[:, :, :key_width].reshape(sp * ctx_rows, key_width)
        ctx_v_ = ctx_kv[:, :, key_width:].reshape(sp * ctx_rows, key_width)
        place = s * total + hb * half - WIN + k_pos
        allowed = jnp.logical_and(
            in_window, jnp.logical_and(place >= 0, place < sp * total)
        )
        q = queries[hb]
        near_s = lax.dot_general(q, band_k, contract, preferred_element_type=f32)
        near_s = jnp.where(allowed, near_s, neg_large)
        ctx_s = lax.dot_general(q, ctx_k, contract, preferred_element_type=f32)
        top = jnp.maximum(
            jnp.max(near_s, axis=-1, keepdims=True), jnp.max(ctx_s, axis=-1, keepdims=True)
        )
        top = jnp.maximum(top, sinks)
        near_e = jnp.exp(near_s - top)
        ctx_e = jnp.exp(ctx_s - top)
        bottom = (
            jnp.sum(near_e, axis=-1, keepdims=True)
            + jnp.sum(ctx_e, axis=-1, keepdims=True)
            + jnp.exp(sinks - top)
        )
        share = 1.0 / bottom
        result = jnp.dot(
            (near_e * share).astype(bf16), band_v, preferred_element_type=f32
        ) + jnp.dot((ctx_e * share).astype(bf16), ctx_v_, preferred_element_type=f32)
        for v in range(query_width // 128):
            sides = []
            for at in range(2):
                h = 2 * v + at
                lanes = result[h * half : (h + 1) * half]
                if h // group != at:
                    lanes = pltpu.roll(lanes, HD, 1)
                sides.append(lanes)
            att_all[p, t, n * half : (n + 1) * half, v * 128 : (v + 1) * 128] = jnp.where(
                low[:half], sides[0], sides[1]
            ).astype(bf16)

    def hand_on(b):
        for j in range(1, chips):
            att_far(b, j).wait_recv()
            att_fwd(b, j).start()

    def out_place(hb, source):
        return blended.at[
            pl.ds(pl.multiple_of(lax.rem(hb, 2) * half, half), half),
            pl.ds(pl.multiple_of(source * out_width, 128), out_width),
        ]

    def out_copy(hb):
        return remote(
            out_cols.at[hb],
            out_place(hb, t),
            out_send.at[hb],
            out_recv.at[2 * t + lax.rem(hb, 2)],
            "tp",
            hb // 2,
        )

    def own_copy(hb):
        return pltpu.make_async_copy(
            out_cols.at[hb],
            out_place(hb, t),
            load_sem.at[len(loads) + 1 + lax.rem(hb, 2)],
        )

    def finish(b):
        att_pair(b).wait_recv()
        for j in range(1, chips):
            att_fwd(b, j).wait_recv()
        sums = jnp.dot(att_all[b, 0], wo[0:query_width], preferred_element_type=f32)
        for i in range(1, tp):
            sums = sums + jnp.dot(
                att_all[b, i],
                wo[i * query_width : (i + 1) * query_width],
                preferred_element_type=f32,
            )
        for n, hb in enumerate(halves_at(b)):
            out_cols[hb] = sums[n * half : (n + 1) * half].astype(bf16)

            @pl.when(hb // 2 == t)
            def _():
                own_copy(hb).start()

            @pl.when(hb // 2 != t)
            def _():
                out_copy(hb).start()

    def attend_step(step, carry):
        @pl.when(step < tp)
        def _():
            @pl.when(step == tp - 2)
            def _():
                halo_right.wait_recv()
                halo_left.wait_recv()

            for n, hb in enumerate(halves_at(step)):
                attend(step, n, hb)
            for j in range(1, chips):
                att_far(step, j).start()
            att_pair(step).start()

        @pl.when(jnp.logical_and(step >= 1, step < tp + 1))
        def _():
            hand_on(step - 1)

        @pl.when(step >= 2)
        def _():
            finish(step - 2)

        return carry

    lax.fori_loop(0, tp + 2, attend_step, 0)

    near.wait_send()
    for copy in far.values():
        copy.wait_send()
    for j in range(1, chips):
        for c in range(PIECES):
            fwd(j, c).wait_send()
    gate_store.wait()
    halo_right.wait_send()
    halo_left.wait_send()
    for b in range(tp):
        att_pair(b).wait_send()
        for j in range(1, chips):
            att_far(b, j).wait_send()
            att_fwd(b, j).wait_send()
    for n in range(2):
        own_copy(2 * t + n).wait()
        for k in range(1, tp):
            other = lax.rem(t + k, tp)
            out_copy(2 * other + n).wait_send()
            remote(
                out_cols.at[2 * other + n],
                out_place(2 * t + n, other),
                out_send.at[2 * other + n],
                out_recv.at[2 * other + n],
                "tp",
                other,
            ).wait_recv()


def local(
    latent,
    context,
    conditioning,
    norm_gain,
    shift_weight,
    scale_weight,
    gate_weight,
    query_weight,
    key_weight,
    value_weight,
    out_weight,
    sink_logit,
):
    tp, sp = lax.axis_size("tp"), lax.axis_size("sp")
    rows, width = latent.shape
    ctx_rows = context.shape[0]
    mod_rows, mod_cols = shift_weight.shape
    query_width, key_width = query_weight.shape[1], key_weight.shape[1]
    out_width = out_weight.shape[1]
    fits = (
        rows == WIN
        and key_width == 2 * HD
        and tp % 2 == 0
        and tp >= 4
        and sp >= 2
        and ctx_rows % NORM_ROWS == 0
        and mod_cols % 128 == 0
    )
    if not fits:
        return local_plain(
            latent,
            context,
            conditioning,
            norm_gain,
            shift_weight,
            scale_weight,
            gate_weight,
            query_weight,
            key_weight,
            value_weight,
            out_weight,
            sink_logit,
        )
    f32, bf16 = jnp.float32, jnp.bfloat16
    chips = tp // 2
    far = (chips - 1) * PIECES
    dma = pltpu.SemaphoreType.DMA
    anywhere = pl.BlockSpec(memory_space=pl.ANY)
    blended, gate = pl.pallas_call(
        functools.partial(fused_kernel, tp, sp),
        out_shape=(
            jax.ShapeDtypeStruct((rows, width), bf16),
            jax.ShapeDtypeStruct((1, width), f32),
        ),
        in_specs=[anywhere] * 11 + [pl.BlockSpec(memory_space=pltpu.SMEM)],
        out_specs=(anywhere, anywhere),
        scratch_shapes=[
            pltpu.VMEM((mod_rows,), bf16),
            pltpu.VMEM((1, width), f32),
            pltpu.VMEM((3, mod_rows, mod_cols), bf16),
            pltpu.VMEM(query_weight.shape, bf16),
            pltpu.VMEM(key_weight.shape, bf16),
            pltpu.VMEM(value_weight.shape, bf16),
            pltpu.VMEM(out_weight.shape, bf16),
            pltpu.VMEM(context.shape, bf16),
            pltpu.VMEM((tp, rows, width), bf16),
            pltpu.VMEM((2 * rows, width), bf16),
            pltpu.VMEM((sp, 1, 3 * mod_cols), f32),
            pltpu.VMEM((tp, 1, 3 * mod_cols), f32),
            pltpu.VMEM((1, width), f32),
            pltpu.VMEM((1, width), f32),
            pltpu.VMEM((1, width), f32),
            pltpu.VMEM((tp, rows, 128), f32),
            pltpu.VMEM((tp, rows, 128), f32),
            pltpu.VMEM((2 * tp, query_width // HD * (rows // 2), key_width), bf16),
            pltpu.VMEM(((tp + 2) * rows, 2 * key_width), bf16),
            pltpu.VMEM((sp, ctx_rows, 2 * key_width), bf16),
            pltpu.VMEM((tp, tp, rows, query_width), bf16),
            pltpu.VMEM((2 * tp, rows // 2, out_width), bf16),
            dma((14,)),
            dma((1,)),
            dma((1,)),
            dma((far,)),
            dma((far,)),
            dma((far,)),
            dma((far,)),
            dma((sp - 1,)),
            dma((sp - 1,)),
            dma((tp - 1,)),
            dma((tp - 1,)),
            dma((sp - 1,)),
            dma((sp - 1,)),
            dma((2,)),
            dma((2,)),
            dma((tp,)),
            dma((tp,)),
            dma((tp * (chips - 1),)),
            dma((tp * (chips - 1),)),
            dma((tp * (chips - 1),)),
            dma((tp * (chips - 1),)),
            dma((2 * tp,)),
            dma((2 * tp,)),
        ],
        compiler_params=pltpu.CompilerParams(
            collective_id=0, has_side_effects=True, vmem_limit_bytes=60 * 1024 * 1024
        ),
        name="fused",
    )(
        latent,
        context,
        conditioning,
        norm_gain.reshape(1, width),
        shift_weight,
        scale_weight,
        gate_weight,
        query_weight,
        key_weight,
        value_weight,
        out_weight,
        sink_logit,
    )
    return (latent.astype(f32) + gate * blended.astype(f32)).astype(bf16)


def solution(mesh):
    in_specs = (
        P(("grp", "sp", "tp"), None),
        P(("grp", "sp"), None),
        P(("grp", "sp")),
        P(),
        P("sp", "tp"),
        P("sp", "tp"),
        P("sp", "tp"),
        P(None, "tp"),
        P(None, "tp"),
        P(None, "tp"),
        P(None, "tp"),
        P("tp"),
    )
    out_specs = P(("grp", "sp", "tp"), None)
    return jax.shard_map(local, mesh=mesh, in_specs=in_specs, out_specs=out_specs, check_vma=False)
```

profile of v0, /device:TPU:0, one launch (start us, length us, event | category | flops | bytes accessed | tf_op | source)
XLA Modules:
  0.0 66.5 jit_solution(15778867218094147295)
XLA Ops:
  0.0 0.0 copy-start
  0.0 64.0 %fused.1 = (bf16[128,4096]{1,0:T(8,128)(2,1)}, f32[1,4096]{1,0:T(1,128)}) custom-call(bf16[128,4096]{1,0:T(8,128)(2,1)} %latent.1, bf16[192,4096]{1,0:T(8,128)(2,1)} %context.1, bf16[1024]{0:T(1024)(128)(2,1)} %conditioning.1, f32[1,4096]{1,0:T(1,128)} %bitcast.3, bf16[1024,1024]{1,0:T(8,128)(2,1)} %shift_weight.1, bf16[1024,1024]{1,0:T(8,128)(2,1)} %scale_weight.1, ...), custom_call_target="tpu_custom_call" | custom-call | tf_op jit(solution)/shard_map/fused/pallas_call | solution.py:792
  64.0 0.0 copy-done
  64.0 2.5 %add_convert_fusion = bf16[128,4096]{1,0:T(8,128)(2,1)} fusion(bf16[128,4096]{1,0:T(8,128)(2,1)} %get-tuple-element.8, bf16[128,4096]{1,0:T(8,128)(2,1)S(1)} %copy-done, f32[4096]{0:T(1024)} %bitcast.2), kind=kLoop, calls=%fused_computation | loop fusion | flops 2621440 | bytes 3162112 | tf_op jit(solution)/shard_map/convert_element_type | solution.py:865
Async XLA Ops:
  0.0 64.0 %copy-start = (bf16[128,4096]{1,0:T(8,128)(2,1)S(1)}, bf16[128,4096]{1,0:T(8,128)(2,1)}, u32[]{:S(2)}) copy-start(bf16[128,4096]{1,0:T(8,128)(2,1)} %latent.1) | copy-start | bytes 3145732
where the time goes:
time: 66.7 us; the launch traced here: 66.5 us
  Pallas kernels  64 us (96%)
  other arithmetic  2.51 us (4%)
    pallas_call x1, Pallas kernels, local(): pl.pallas_call(functools.partial(fused_kernel, tp, sp), out_shape=(jax.Sh...  64 us
    convert_element_type x1, other arithmetic, local(): return (latent.astype(f32) + gate * blended.astype(f32)).astype(bf16)  2.51 us

commit v1 on v0

v1 whole, which is shorter than its diff:
```python
import functools

import jax
import jax.numpy as jnp
from jax import lax
from jax.experimental import pallas as pl
from jax.experimental.pallas import tpu as pltpu
from jax.sharding import PartitionSpec as P

HEADS = 16
KV_HEADS = 8
HD = 64
GRID_W = 64
WIN = 128


epsilon = 1e-06
rope_base = 10000.0
neg_large = -1e30


def with_halo(cells, sides, width):
    for axis, dim in sides:
        count = lax.axis_size(axis)
        ends = count - 1
        head = lax.slice_in_dim(cells, 0, width, axis=dim)
        tail = lax.slice_in_dim(cells, cells.shape[dim] - width, cells.shape[dim], axis=dim)
        cells = jnp.concatenate(
            [
                lax.ppermute(tail, axis, [(i, (i + 1) % count) for i in range(ends)]),
                cells,
                lax.ppermute(head, axis, [((i + 1) % count, i) for i in range(ends)]),
            ],
            axis=dim,
        )
    return cells


def row_norm(matrix, norm_gain):
    values = matrix.astype(jnp.float32)
    return (
        values * lax.rsqrt(jnp.mean(values * values, axis=-1, keepdims=True) + epsilon) * norm_gain
    )


def axial_turn(values, position):
    half_dim = values.shape[-1] // 2
    quarter = half_dim // 2
    inverse = rope_base ** (-jnp.arange(quarter, dtype=jnp.float32) / quarter)

    def turn(section, coordinate):
        angles = coordinate.astype(jnp.float32)[:, None] * inverse[None, :]
        cosine = jnp.cos(angles)[:, None, :]
        sine_part = jnp.sin(angles)[:, None, :]
        leading = section[..., :quarter]
        trailing = section[..., quarter:]
        return jnp.concatenate(
            [leading * cosine - trailing * sine_part, leading * sine_part + trailing * cosine],
            axis=-1,
        )

    return jnp.concatenate(
        [
            turn(values[..., :half_dim], position // GRID_W),
            turn(values[..., half_dim:], position % GRID_W),
        ],
        axis=-1,
    )


def context_pairs(context_rows, norm_gain, key_weight, value_weight):
    prepared = row_norm(context_rows, norm_gain).astype(jnp.bfloat16)
    return jnp.concatenate(
        [
            jnp.dot(prepared, key_weight, preferred_element_type=jnp.float32),
            jnp.dot(prepared, value_weight, preferred_element_type=jnp.float32),
        ],
        axis=1,
    ).astype(jnp.bfloat16)


def local_plain(
    latent,
    context,
    conditioning,
    norm_gain,
    shift_weight,
    scale_weight,
    gate_weight,
    query_weight,
    key_weight,
    value_weight,
    out_weight,
    sink_logit,
):
    lifted = jax.nn.silu(conditioning.astype(jnp.float32)).astype(jnp.bfloat16)[None, :]
    shift_part = jnp.dot(lifted, shift_weight, preferred_element_type=jnp.float32)[0]
    scale_part = jnp.dot(lifted, scale_weight, preferred_element_type=jnp.float32)[0]
    gate_part = jnp.dot(lifted, gate_weight, preferred_element_type=jnp.float32)[0]
    summed = lax.psum((shift_part, scale_part, gate_part), "sp")
    shift_vec, scale_vec, gate_vec = (
        lax.all_gather(summed[0], "tp", axis=0, tiled=True),
        lax.all_gather(summed[1], "tp", axis=0, tiled=True),
        lax.all_gather(summed[2], "tp", axis=0, tiled=True),
    )
    normed = (row_norm(latent, norm_gain) * (1.0 + scale_vec) + shift_vec).astype(jnp.bfloat16)
    segment = lax.all_gather(normed, "tp", axis=0, tiled=True)
    projected = jnp.concatenate(
        [
            jnp.dot(segment, query_weight, preferred_element_type=jnp.float32),
            jnp.dot(segment, key_weight, preferred_element_type=jnp.float32),
            jnp.dot(segment, value_weight, preferred_element_type=jnp.float32),
        ],
        axis=1,
    )
    row_count = projected.shape[0]
    query_width = query_weight.shape[1]
    key_width = key_weight.shape[1]
    query_heads = query_width // HD
    pair_heads = key_width // HD
    group_size = HEADS // KV_HEADS
    row_offset = lax.axis_index("sp") * row_count
    position = row_offset + jnp.arange(row_count, dtype=jnp.int32)
    queries = axial_turn(
        projected[:, :query_width].reshape(row_count, query_heads, HD), position
    ).astype(jnp.bfloat16)
    latent_keys = axial_turn(
        projected[:, query_width : query_width + key_width].reshape(row_count, pair_heads, HD),
        position,
    ).astype(jnp.bfloat16)
    latent_values = projected[:, query_width + key_width :].astype(jnp.bfloat16)
    key_value = jnp.concatenate([latent_keys.reshape(row_count, key_width), latent_values], axis=1)
    widened = with_halo(key_value, (("sp", 0),), WIN)
    context_all = lax.all_gather(
        context_pairs(context, norm_gain, key_weight, value_weight), "sp", axis=0, tiled=True
    )
    block_count = row_count // WIN
    context_count = context_all.shape[0]
    query_blocks = queries.reshape(block_count, WIN, pair_heads, group_size, HD)
    band_blocks = widened.reshape(block_count + 2, WIN, 2 * key_width)
    band_rows = jnp.concatenate(
        [band_blocks[:block_count], band_blocks[1 : block_count + 1], band_blocks[2:]], axis=1
    )
    band_keys = band_rows[..., :key_width].reshape(block_count, 3 * WIN, pair_heads, HD)
    band_values = band_rows[..., key_width:].reshape(block_count, 3 * WIN, pair_heads, HD)
    context_keys = context_all[:, :key_width].reshape(context_count, pair_heads, HD)
    context_values = context_all[:, key_width:].reshape(context_count, pair_heads, HD)
    factor = HD ** (-0.5)
    local_scores = (
        jnp.einsum("nqhgd,nkhd->nhgqk", query_blocks, band_keys, preferred_element_type=jnp.float32)
        * factor
    )
    query_pos = position.reshape(block_count, WIN)
    key_pos = (
        row_offset
        - WIN
        + jnp.arange(block_count, dtype=jnp.int32)[:, None] * WIN
        + jnp.arange(3 * WIN, dtype=jnp.int32)[None, :]
    )
    seq_total = row_count * lax.axis_size("sp")
    allowed = (
        (jnp.abs(key_pos[:, None, :] - query_pos[:, :, None]) <= WIN)
        & (key_pos[:, None, :] >= 0)
        & (key_pos[:, None, :] < seq_total)
    )
    local_scores = jnp.where(allowed[:, None, None], local_scores, neg_large)
    context_scores = (
        jnp.einsum(
            "nqhgd,thd->nhgqt", query_blocks, context_keys, preferred_element_type=jnp.float32
        )
        * factor
    )
    sink_values = sink_logit.reshape(pair_heads, group_size)[None, :, :, None, None]
    highest = jnp.maximum(
        jnp.maximum(
            jnp.max(local_scores, axis=-1, keepdims=True),
            jnp.max(context_scores, axis=-1, keepdims=True),
        ),
        sink_values,
    )
    local_exp = jnp.exp(local_scores - highest)
    context_exp = jnp.exp(context_scores - highest)
    denominator = (
        jnp.sum(local_exp, axis=-1, keepdims=True)
        + jnp.sum(context_exp, axis=-1, keepdims=True)
        + jnp.exp(sink_values - highest)
    )
    local_weights = (local_exp / denominator).astype(jnp.bfloat16)
    context_weights = (context_exp / denominator).astype(jnp.bfloat16)
    attended = jnp.einsum(
        "nhgqk,nkhd->nqhgd", local_weights, band_values, preferred_element_type=jnp.float32
    ) + jnp.einsum(
        "nhgqt,thd->nqhgd", context_weights, context_values, preferred_element_type=jnp.float32
    )
    attended = attended.reshape(row_count, query_width).astype(jnp.bfloat16)
    columns_part = jnp.dot(
        lax.all_gather(attended, "tp", axis=1, tiled=True),
        out_weight,
        preferred_element_type=jnp.float32,
    ).astype(jnp.bfloat16)
    blended = lax.all_to_all(columns_part, "tp", split_axis=0, concat_axis=1, tiled=True)
    return (latent.astype(jnp.float32) + gate_vec * blended.astype(jnp.float32)).astype(
        jnp.bfloat16
    )


LATENT_CHUNKS = 8
WEIGHT_CHUNKS = 4
AHEAD = 3
NORM_ROWS = 16


def remote(src, dst, send, recv, device):
    return pltpu.make_async_remote_copy(
        src_ref=src,
        dst_ref=dst,
        send_sem=send,
        recv_sem=recv,
        device_id=device,
        device_id_type=pl.DeviceIdType.MESH,
    )


def fused_kernel(
    sp,
    latent,
    context,
    conditioning,
    norm_gain,
    shift_weight,
    scale_weight,
    gate_weight,
    query_weight,
    key_weight,
    value_weight,
    out_weight,
    sink,
    mixed,
    cond_v,
    gain_v,
    mod_w,
    proj_w,
    wo,
    ctx_v,
    lat_own,
    lat_far,
    normed,
    stat_out,
    stat_in,
    row_scale,
    sink_v,
    mod_part,
    mod_all,
    factor_v,
    shift_v,
    gate_v,
    turn_cos,
    turn_sin,
    acc,
    queries,
    key_value,
    ctx_kv,
    att,
    att_out,
    out_part,
    mixed_v,
    load_sem,
    lat_send,
    lat_recv,
    stat_sem,
    pair_send,
    pair_recv,
    wox_send,
    wo_send,
    wo_recv,
    woy_send,
    woy_recv,
    wop_send,
    wop_recv,
    modz_send,
    modz_recv,
    modt_send,
    modt_recv,
    ctxz_send,
    ctxz_recv,
    ctxp_sem,
    kv_send,
    kv_recv,
    halo_sem,
    att_send,
    att_recv,
):
    g = lax.axis_index("grp")
    s = lax.axis_index("sp")
    t = lax.axis_index("tp")
    chip = t // 2
    core = lax.rem(t, 2)
    pair = chip * 2 + 1 - core
    far = (1 - chip) * 2 + core
    pair_dev, far_dev, y_dev = {"tp": pair}, {"tp": far}, {"grp": 1 - g}
    right_dev = {"sp": lax.rem(s + 1, sp)}
    left_dev = {"sp": lax.rem(s + sp - 1, sp)}
    has_right, has_left = s < sp - 1, s > 0
    rows, width = latent.shape
    ctx_rows = context.shape[0]
    mod_cols = shift_weight.shape[1]
    qw = query_weight.shape[1]
    kw = key_weight.shape[1]
    heads = qw // HD
    group = heads // (kw // HD)
    tp = 4
    total = tp * rows
    out_rows, out_width = out_weight.shape
    half = rows // 2
    f32, bf16 = jnp.float32, jnp.bfloat16
    chunk = width // LATENT_CHUNKS
    shard = out_rows // (2 * sp)
    slab = shard // WEIGHT_CHUNKS
    MESH = pl.DeviceIdType.MESH

    loads = [
        (latent, lat_own),
        (conditioning, cond_v),
        (shift_weight, mod_w.at[0]),
        (scale_weight, mod_w.at[1]),
        (gate_weight, mod_w.at[2]),
        (norm_gain, gain_v),
        (context, ctx_v),
        (key_weight, proj_w.at[core, :, qw : qw + kw]),
        (value_weight, proj_w.at[core, :, qw + kw : qw + 2 * kw]),
        (query_weight, proj_w.at[core, :, 0:qw]),
        (out_weight, wo.at[t]),
    ]
    loads = [pltpu.make_async_copy(a, b, load_sem.at[i]) for i, (a, b) in enumerate(loads)]
    for load in loads:
        load.start()

    barrier = pltpu.get_barrier_semaphore()
    for k in range(1, tp):
        pl.semaphore_signal(
            barrier, inc=1, device_id={"tp": lax.rem(t + k, tp)}, device_id_type=MESH
        )
    pl.semaphore_signal(barrier, inc=1, device_id=y_dev, device_id_type=MESH)
    for has, place in ((has_right, right_dev), (has_left, left_dev)):

        @pl.when(has)
        def _():
            for peer in (t, pair):
                pl.semaphore_signal(
                    barrier, inc=1, device_id={**place, "tp": peer}, device_id_type=MESH
                )

    lane = lax.broadcasted_iota(jnp.int32, (rows, 128), 1)
    row = lax.broadcasted_iota(jnp.int32, (rows, 128), 0)
    diagonal = lane == row

    loads[0].wait()

    def row_stat(i, carry):
        part = pl.ds(pl.multiple_of(i * NORM_ROWS, NORM_ROWS), NORM_ROWS)
        values = lat_own[part].astype(f32)
        scale = lax.rsqrt(jnp.mean(values * values, axis=-1, keepdims=True) + epsilon)
        row_scale[0, part] = jnp.broadcast_to(scale, (NORM_ROWS, 128))
        return carry

    lax.fori_loop(0, rows // NORM_ROWS, row_stat, 0)
    flat = jnp.sum(jnp.where(diagonal, row_scale[0], 0.0), axis=0, keepdims=True)
    stat_out[...] = jnp.broadcast_to(flat, (8, 128))
    sink_row = lax.broadcasted_iota(jnp.int32, (8, 128), 0)
    sink_all = jnp.full((8, 128), sink[0], f32)
    for h in range(1, heads):
        sink_all = jnp.where(sink_row == h, sink[h], sink_all)
    sink_v[core] = sink_all

    pl.semaphore_wait(
        barrier, tp + jnp.where(has_right, 2, 0) + jnp.where(has_left, 2, 0)
    )

    def lat_copy(j):
        cols = pl.ds(pl.multiple_of(j * chunk, 128), chunk)
        return remote(
            latent.at[:, cols], lat_far.at[:, cols], lat_send.at[j], lat_recv.at[j], far_dev
        )

    def wo_rows(gg, j, c):
        return pl.ds(pl.multiple_of((gg * sp + j) * shard + c * slab, 16), slab)

    def wo_cross(c):
        part = wo_rows(g, s, c)
        return remote(
            out_weight.at[part], wo.at[t, part], wox_send.at[c], wo_recv.at[s, c], far_dev
        )

    stat_copy = remote(stat_out, stat_in, stat_sem.at[0], stat_sem.at[1], far_dev)
    stat_copy.start()
    for c in range(WEIGHT_CHUNKS):
        wo_cross(c).start()
    for j in range(AHEAD):
        lat_copy(j).start()
    pair_copies = [
        (sink_v.at[core], sink_v.at[core]),
        (query_weight, proj_w.at[core, :, 0:qw]),
        (key_weight, proj_w.at[core, :, qw : qw + kw]),
        (value_weight, proj_w.at[core, :, qw + kw : qw + 2 * kw]),
        (out_weight, wo.at[t]),
    ]
    pair_copies = [
        remote(a, b, pair_send.at[i], pair_recv.at[i], pair_dev)
        for i, (a, b) in enumerate(pair_copies)
    ]
    for copy in pair_copies:
        copy.start()

    def line_copy(at, j, send, recv, toward):
        return remote(at(j), at(j), send.at[toward, j], recv.at[j], (left_dev, right_dev)[toward])

    def line_start(at, send, recv):
        for toward, has in ((0, has_left), (1, has_right)):

            @pl.when(has)
            def _():
                line_copy(at, s, send, recv, toward).start()

    def line_relay(k, at, send, recv):
        for toward, has, j, there in (
            (1, has_right, s - k, s >= k),
            (0, has_left, s + k, s + k < sp),
        ):

            @pl.when(there)
            def _():
                line_copy(at, j, send, recv, toward).wait_recv()

                @pl.when(has)
                def _():
                    line_copy(at, j, send, recv, toward).start()

    def line_finish(at, send, recv):
        for j in range(sp):
            for toward, has, sent in ((1, has_right, j <= s), (0, has_left, j >= s)):

                @pl.when(jnp.logical_and(has, sent))
                def _():
                    line_copy(at, j, send, recv, toward).wait_send()

    def mod_at(j):
        return mod_part.at[j]

    def ctx_at(j):
        return ctx_kv.at[core, pl.ds(pl.multiple_of(j * ctx_rows, 16), ctx_rows)]

    for i in range(1, 5):
        loads[i].wait()
    cond = cond_v[...].astype(f32).reshape(1, cond_v.shape[0])
    lifted = jnp.broadcast_to(cond / (1.0 + jnp.exp(-cond)), (16, cond.shape[1])).astype(bf16)
    for i in range(3):
        mod_part[s, :, i * mod_cols : (i + 1) * mod_cols] = jnp.dot(
            lifted, mod_w[i], preferred_element_type=f32
        )[0:1]
    line_start(mod_at, modz_send, modz_recv)

    for i in range(5, 9):
        loads[i].wait()

    def norm_context(i, carry):
        part = pl.ds(pl.multiple_of(i * NORM_ROWS, NORM_ROWS), NORM_ROWS)
        values = ctx_v[part].astype(f32)
        scale = lax.rsqrt(jnp.mean(values * values, axis=-1, keepdims=True) + epsilon)
        ctx_v[part] = (values * scale * gain_v[...]).astype(bf16)
        return carry

    lax.fori_loop(0, ctx_rows // NORM_ROWS, norm_context, 0)
    own_ctx = pl.ds(pl.multiple_of(s * ctx_rows, 16), ctx_rows)
    ctx_kv[core, own_ctx] = jnp.dot(
        ctx_v[...], proj_w[core, :, qw : qw + 2 * kw], preferred_element_type=f32
    ).astype(bf16)
    line_relay(1, mod_at, modz_send, modz_recv)
    line_start(ctx_at, ctxz_send, ctxz_recv)

    def wo_line(j, c, toward):
        part = wo.at[far, wo_rows(g, j, c)]
        return remote(
            part, part, wo_send.at[toward, j, c], wo_recv.at[j, c], (left_dev, right_dev)[toward]
        )

    def wo_across(j, c):
        part = wo.at[far, wo_rows(g, j, c)]
        return remote(part, part, woy_send, woy_recv, y_dev)

    def wo_own(c):
        wo_line(s, c, 0).wait_recv()
        for toward, has in ((0, has_left), (1, has_right)):

            @pl.when(has)
            def _():
                wo_line(s, c, toward).start()

        wo_across(s, c).start()

    def wo_relay(e):
        k, c = e // WEIGHT_CHUNKS, lax.rem(e, WEIGHT_CHUNKS)
        for toward, has, j, there in (
            (1, has_right, s - k, s >= k),
            (0, has_left, s + k, s + k < sp),
        ):

            @pl.when(there)
            def _():
                wo_line(j, c, toward).wait_recv()

                @pl.when(has)
                def _():
                    wo_line(j, c, toward).start()

                wo_across(j, c).start()

    def wo_relays(low, high):
        def step(e, carry):
            wo_relay(e)
            return carry

        lax.fori_loop(low, high, step, 0)

    quarter = HD // 4
    inverse = jnp.exp(
        lax.rem(lane, quarter).astype(f32) * (-jnp.log(jnp.float32(rope_base)) / quarter)
    )
    first = lax.rem(lane, 2 * quarter) < quarter
    by_row = lax.rem(lane, HD) < HD // 2

    def tables(b, carry):
        place = s * total + jnp.where(b == 0, t, far) * rows + row
        coordinate = jnp.where(by_row, place // GRID_W, lax.rem(place, GRID_W))
        angles = coordinate.astype(f32) * inverse
        turn_cos[b] = jnp.cos(angles)
        sines = jnp.sin(angles)
        turn_sin[b] = jnp.where(first, -sines, sines)
        return carry

    wo_own(0)
    line_relay(2, mod_at, modz_send, modz_recv)
    lax.fori_loop(0, 2, tables, 0)
    wo_own(1)
    line_relay(1, ctx_at, ctxz_send, ctxz_recv)
    for k in range(3, sp):
        line_relay(k, mod_at, modz_send, modz_recv)
    summed = mod_part[0]
    for k in range(1, sp):
        summed = summed + mod_part[k]
    mod_all[t] = summed
    mods = []
    for k in range(1, tp):
        copy = remote(
            mod_all.at[t],
            mod_all.at[t],
            modt_send.at[k - 1],
            modt_recv.at[k - 1],
            {"tp": lax.rem(t + k, tp)},
        )
        copy.start()
        mods.append(copy)
    for c in range(2, WEIGHT_CHUNKS):
        wo_own(c)
    line_relay(2, ctx_at, ctxz_send, ctxz_recv)
    wo_relays(WEIGHT_CHUNKS, 2 * WEIGHT_CHUNKS)
    for k in range(3, sp):
        line_relay(k, ctx_at, ctxz_send, ctxz_recv)
    ctx_pair = remote(ctx_kv.at[core], ctx_kv.at[core], ctxp_sem.at[0], ctxp_sem.at[1], pair_dev)
    ctx_pair.start()

    stat_copy.wait_recv()
    column = jnp.sum(
        jnp.where(diagonal, jnp.broadcast_to(stat_in[0:1], (rows, 128)), 0.0), axis=1, keepdims=True
    )
    row_scale[1] = jnp.broadcast_to(column, (rows, 128))

    for copy in mods:
        copy.wait_recv()
    for i in range(tp):
        cols = slice(i * mod_cols, (i + 1) * mod_cols)
        shift_v[:, cols] = mod_all[i, :, 0:mod_cols]
        factor_v[:, cols] = gain_v[:, cols] * (1.0 + mod_all[i, :, mod_cols : 2 * mod_cols])
        gate_v[:, cols] = mod_all[i, :, 2 * mod_cols : 3 * mod_cols]

    def project(j, block, source):
        cols = pl.ds(pl.multiple_of(j * chunk, 128), chunk)

        def norm_rows(i, carry):
            part = pl.ds(pl.multiple_of(i * NORM_ROWS, NORM_ROWS), NORM_ROWS)
            values = source[part, cols].astype(f32)
            scale = row_scale[block, part, 0:1]
            normed[part] = (values * scale * factor_v[:, cols] + shift_v[:, cols]).astype(bf16)
            return carry

        lax.fori_loop(0, rows // NORM_ROWS, norm_rows, 0)
        for slot in range(2):
            product = jnp.dot(
                normed[...], proj_w[slot, cols], preferred_element_type=f32
            )

            @pl.when(j == 0)
            def _():
                acc[slot] = product

            @pl.when(j != 0)
            def _():
                acc[slot] = acc[slot] + product

    low = lane < HD

    def finish_projection(block, position):
        cosine, sine = turn_cos[block], turn_sin[block]

        def turned(values):
            swapped = jnp.where(
                first, pltpu.roll(values, 128 - quarter, 1), pltpu.roll(values, quarter, 1)
            )
            return values * cosine + swapped * sine

        factor = HD ** (-0.5)
        base = pl.ds(pl.multiple_of(position * rows, rows), rows)
        for slot in range(2):
            key_value[slot, base, 0:kw] = turned(acc[slot, :, qw : qw + kw]).astype(bf16)
            key_value[slot, base, kw : 2 * kw] = acc[slot, :, qw + kw : qw + 2 * kw].astype(bf16)
            for h in range(heads):
                lanes = acc[slot, :, (h // 2) * 128 : (h // 2 + 1) * 128]
                lanes = turned(lanes).astype(bf16).astype(f32) * factor
                at, want = h % 2, h // group
                if at != want:
                    lanes = pltpu.roll(lanes, HD, 1)
                keep = low if want == 0 else jnp.logical_not(low)
                lanes = jnp.where(keep, lanes, 0.0).astype(bf16)
                for n in range(2):
                    queries[block, n, slot, h * half : (h + 1) * half] = lanes[
                        n * half : (n + 1) * half
                    ]

    def kv_at(position):
        return key_value.at[:, pl.ds(pl.multiple_of(position * rows, rows), rows)]

    def kv_pair(block, position):
        return remote(
            kv_at(position), kv_at(position), kv_send.at[block], kv_recv.at[block], pair_dev
        )

    halo_down = remote(
        kv_at(1), kv_at(tp + 1), halo_sem.at[0], halo_sem.at[1], {**left_dev, "tp": pair}
    )
    halo_up = remote(kv_at(tp), kv_at(0), halo_sem.at[0], halo_sem.at[1], {**right_dev, "tp": pair})
    sends_down = jnp.logical_and(core == 0, has_left)
    sends_up = jnp.logical_and(core == 1, has_right)

    def send_halo(mine):
        @pl.when(jnp.logical_and(mine, sends_down))
        def _():
            halo_down.start()

        @pl.when(jnp.logical_and(mine, sends_up))
        def _():
            halo_up.start()

    def wait_halo(mine):
        @pl.when(jnp.logical_and(mine, sends_down))
        def _():
            halo_up.wait_recv()

        @pl.when(jnp.logical_and(mine, sends_up))
        def _():
            halo_down.wait_recv()

    edge = jnp.zeros((2, rows, 2 * kw), bf16)

    @pl.when(jnp.logical_and(core == 0, jnp.logical_not(has_left)))
    def _():
        key_value[:, 0:rows] = edge

    @pl.when(jnp.logical_and(core == 1, jnp.logical_not(has_right)))
    def _():
        key_value[:, (tp + 1) * rows : (tp + 2) * rows] = edge

    for i in range(9, 11):
        loads[i].wait()
    for copy in pair_copies[0:4]:
        copy.wait_recv()

    def own_step(j, carry):
        project(j, 0, lat_own)
        return carry

    lax.fori_loop(0, LATENT_CHUNKS, own_step, 0)
    finish_projection(0, t + 1)
    kv_pair(0, t + 1).start()
    send_halo(chip == core)

    def far_step(j, carry):
        @pl.when(j < 4)
        def _():
            wo_relays(2 * WEIGHT_CHUNKS + 2 * j, 2 * WEIGHT_CHUNKS + 2 * j + 2)

        lat_copy(j).wait_recv()

        @pl.when(j + AHEAD < LATENT_CHUNKS)
        def _():
            lat_copy(j + AHEAD).start()

        project(j, 1, lat_far)
        return carry

    lax.fori_loop(0, LATENT_CHUNKS, far_step, 0)
    finish_projection(1, far + 1)
    kv_pair(1, far + 1).start()
    send_halo(chip != core)

    def wo_pair(gg):
        part = wo.at[far, pl.ds(pl.multiple_of(gg * sp * shard, 16), sp * shard)]
        return remote(part, part, wop_send.at[gg], wop_recv.at[gg], pair_dev)

    wo_pair(g).start()

    kv_pair(0, pair + 1).wait_recv()
    ctx_pair.wait_recv()

    contract = (((1,), (1,)), ((), ()))
    band = 2 * WIN + half
    stack = heads * half
    q_pos = lax.rem(lax.broadcasted_iota(jnp.int32, (stack, band), 0), half)
    k_pos = lax.broadcasted_iota(jnp.int32, (stack, band), 1)
    in_window = jnp.logical_and(k_pos >= q_pos, k_pos <= q_pos + 2 * WIN)

    def attend(block, position, n, slot, target):
        start = pl.multiple_of((position - 1) * rows + n * half, half)
        band_k = key_value[slot, pl.ds(start, band), 0:kw]
        band_v = key_value[slot, pl.ds(start, band), kw : 2 * kw]
        ctx_k = ctx_kv[slot, :, 0:kw]
        ctx_v_ = ctx_kv[slot, :, kw : 2 * kw]
        sinks = jnp.concatenate(
            [jnp.broadcast_to(sink_v[slot, h : h + 1, 0:1], (half, 1)) for h in range(heads)],
            axis=0,
        )
        place = s * total + start - WIN + k_pos
        allowed = jnp.logical_and(in_window, jnp.logical_and(place >= 0, place < sp * total))
        q = queries[block, n, slot]
        near_s = lax.dot_general(q, band_k, contract, preferred_element_type=f32)
        near_s = jnp.where(allowed, near_s, neg_large)
        ctx_s = lax.dot_general(q, ctx_k, contract, preferred_element_type=f32)
        top = jnp.maximum(
            jnp.max(near_s, axis=-1, keepdims=True), jnp.max(ctx_s, axis=-1, keepdims=True)
        )
        top = jnp.maximum(top, sinks)
        near_e = jnp.exp(near_s - top)
        ctx_e = jnp.exp(ctx_s - top)
        bottom = (
            jnp.sum(near_e, axis=-1, keepdims=True)
            + jnp.sum(ctx_e, axis=-1, keepdims=True)
            + jnp.exp(sinks - top)
        )
        share = 1.0 / bottom
        result = jnp.dot(
            (near_e * share).astype(bf16), band_v, preferred_element_type=f32
        ) + jnp.dot((ctx_e * share).astype(bf16), ctx_v_, preferred_element_type=f32)
        for v in range(qw // 128):
            sides = []
            for at in range(2):
                h = 2 * v + at
                lanes = result[h * half : (h + 1) * half]
                if h // group != at:
                    lanes = pltpu.roll(lanes, HD, 1)
                sides.append(lanes)
            target[
                slot, pl.ds(pl.multiple_of(n * half, half), half), v * 128 : (v + 1) * 128
            ] = jnp.where(low[:half], sides[0], sides[1]).astype(bf16)

    def att_copy(n):
        part = pl.ds(pl.multiple_of(n * half, half), half)
        return remote(
            att_out.at[:, part], att.at[chip, :, part], att_send.at[n], att_recv.at[n], far_dev
        )

    kv_pair(1, pair + 1).wait_recv()
    wait_halo(chip != core)

    def far_attend(i, carry):
        n, slot = i // 2, lax.rem(i, 2)
        attend(1, far + 1, n, slot, att_out)

        @pl.when(slot == 1)
        def _():
            att_copy(n).start()

        return carry

    lax.fori_loop(0, 4, far_attend, 0)
    wo_gathered = wo.at[far, pl.ds(pl.multiple_of((1 - g) * sp * shard, 16), sp * shard)]
    remote(wo_gathered, wo_gathered, woy_send, woy_recv, y_dev).wait_recv()
    wo_pair(1 - g).start()
    wait_halo(chip == core)

    def own_attend(i, carry):
        n, slot = i // 2, lax.rem(i, 2)
        attend(0, t + 1, n, slot, att.at[chip])
        return carry

    lax.fori_loop(0, 4, own_attend, 0)

    pair_copies[4].wait_recv()

    def out_product(x, i):
        sums = None
        for slot in range(2):
            part = pl.ds(pl.multiple_of((2 * x + slot) * qw, qw), qw)
            product = jnp.dot(att[x, slot], wo[i, part], preferred_element_type=f32)
            sums = product if sums is None else sums + product
        return sums

    order = (t, pair, far, (1 - chip) * 2 + 1 - core)
    other = (1 - chip) * 2 + 1 - core
    for k, i in enumerate(order):
        if k == 3:
            for gg in range(2):
                part = wo.at[other, pl.ds(gg * sp * shard, sp * shard)]
                remote(part, part, wop_send.at[gg], wop_recv.at[gg], pair_dev).wait_recv()
        out_part[k] = out_product(chip, i)
    att_copy(0).wait_recv()
    att_copy(1).wait_recv()
    stores = []
    for k, i in enumerate(order):
        cols = pl.ds(pl.multiple_of(i * out_width, 128), out_width)
        blended = (out_part[k] + out_product(1 - chip, i)).astype(bf16).astype(f32)
        mixed_v[:, cols] = (lat_own[:, cols].astype(f32) + gate_v[:, cols] * blended).astype(bf16)
        store = pltpu.make_async_copy(
            mixed_v.at[:, cols], mixed.at[:, cols], load_sem.at[len(loads) + k]
        )
        store.start()
        stores.append(store)

    stat_copy.wait_send()
    for c in range(WEIGHT_CHUNKS):
        wo_cross(c).wait_send()
    for j in range(LATENT_CHUNKS):
        lat_copy(j).wait_send()
    for copy in pair_copies:
        copy.wait_send()
    for copy in mods:
        copy.wait_send()
    line_finish(mod_at, modz_send, modz_recv)
    line_finish(ctx_at, ctxz_send, ctxz_recv)
    ctx_pair.wait_send()
    for j in range(sp):
        for toward, has, sent in ((1, has_right, j <= s), (0, has_left, j >= s)):

            @pl.when(jnp.logical_and(has, sent))
            def _():
                def step(c, carry):
                    wo_line(j, c, toward).wait_send()
                    return carry

                lax.fori_loop(0, WEIGHT_CHUNKS, step, 0)

    wo_sent = wo.at[far, pl.ds(pl.multiple_of(g * sp * shard, 16), sp * shard)]
    remote(wo_sent, wo_sent, woy_send, woy_recv, y_dev).wait_send()
    wo_pair(0).wait_send()
    wo_pair(1).wait_send()
    kv_pair(0, t + 1).wait_send()
    kv_pair(1, far + 1).wait_send()

    @pl.when(sends_down)
    def _():
        halo_down.wait_send()

    @pl.when(sends_up)
    def _():
        halo_up.wait_send()

    att_copy(0).wait_send()
    att_copy(1).wait_send()
    for store in stores:
        store.wait()


def local(
    latent,
    context,
    conditioning,
    norm_gain,
    shift_weight,
    scale_weight,
    gate_weight,
    query_weight,
    key_weight,
    value_weight,
    out_weight,
    sink_logit,
):
    tp, sp, grp = lax.axis_size("tp"), lax.axis_size("sp"), lax.axis_size("grp")
    rows, width = latent.shape
    ctx_rows = context.shape[0]
    mod_rows, mod_cols = shift_weight.shape
    query_width, key_width = query_weight.shape[1], key_weight.shape[1]
    out_rows, out_width = out_weight.shape
    fits = (
        rows == WIN
        and rows == 128
        and key_width == 2 * HD
        and query_width == 4 * HD
        and tp == 4
        and grp == 2
        and sp >= 3
        and ctx_rows % NORM_ROWS == 0
        and mod_cols % 128 == 0
        and width % (128 * LATENT_CHUNKS) == 0
        and out_width % 128 == 0
        and tp * out_width == width
        and out_rows == tp * query_width
        and out_rows % (2 * sp * WEIGHT_CHUNKS * 16) == 0
    )
    if not fits:
        return local_plain(
            latent,
            context,
            conditioning,
            norm_gain,
            shift_weight,
            scale_weight,
            gate_weight,
            query_weight,
            key_weight,
            value_weight,
            out_weight,
            sink_logit,
        )
    f32, bf16 = jnp.float32, jnp.bfloat16
    dma = pltpu.SemaphoreType.DMA
    anywhere = pl.BlockSpec(memory_space=pl.ANY)
    return pl.pallas_call(
        functools.partial(fused_kernel, sp),
        out_shape=jax.ShapeDtypeStruct((rows, width), bf16),
        in_specs=[anywhere] * 11 + [pl.BlockSpec(memory_space=pltpu.SMEM)],
        out_specs=anywhere,
        scratch_shapes=[
            pltpu.VMEM((mod_rows,), bf16),
            pltpu.VMEM((1, width), f32),
            pltpu.VMEM((3, mod_rows, mod_cols), bf16),
            pltpu.VMEM((2, width, query_width + 2 * key_width), bf16),
            pltpu.VMEM((tp, out_rows, out_width), bf16),
            pltpu.VMEM(context.shape, bf16),
            pltpu.VMEM((rows, width), bf16),
            pltpu.VMEM((rows, width), bf16),
            pltpu.VMEM((rows, width // LATENT_CHUNKS), bf16),
            pltpu.VMEM((8, 128), f32),
            pltpu.VMEM((8, 128), f32),
            pltpu.VMEM((2, rows, 128), f32),
            pltpu.VMEM((2, 8, 128), f32),
            pltpu.VMEM((sp, 1, 3 * mod_cols), f32),
            pltpu.VMEM((tp, 1, 3 * mod_cols), f32),
            pltpu.VMEM((1, width), f32),
            pltpu.VMEM((1, width), f32),
            pltpu.VMEM((1, width), f32),
            pltpu.VMEM((2, rows, 128), f32),
            pltpu.VMEM((2, rows, 128), f32),
            pltpu.VMEM((2, rows, query_width + 2 * key_width), f32),
            pltpu.VMEM((2, 2, 2, query_width // HD * (rows // 2), key_width), bf16),
            pltpu.VMEM((2, (tp + 2) * rows, 2 * key_width), bf16),
            pltpu.VMEM((2, sp * ctx_rows, 2 * key_width), bf16),
            pltpu.VMEM((2, 2, rows, query_width), bf16),
            pltpu.VMEM((2, rows, query_width), bf16),
            pltpu.VMEM((tp, rows, out_width), f32),
            pltpu.VMEM((rows, width), bf16),
            dma((15,)),
            dma((LATENT_CHUNKS,)),
            dma((LATENT_CHUNKS,)),
            dma((2,)),
            dma((5,)),
            dma((5,)),
            dma((WEIGHT_CHUNKS,)),
            dma((2, sp, WEIGHT_CHUNKS)),
            dma((sp, WEIGHT_CHUNKS)),
            dma,
            dma,
            dma((2,)),
            dma((2,)),
            dma((2, sp)),
            dma((sp,)),
            dma((tp - 1,)),
            dma((tp - 1,)),
            dma((2, sp)),
            dma((sp,)),
            dma((2,)),
            dma((2,)),
            dma((2,)),
            dma((2,)),
            dma((2,)),
            dma((2,)),
        ],
        compiler_params=pltpu.CompilerParams(
            collective_id=0, has_side_effects=True, vmem_limit_bytes=60 * 1024 * 1024
        ),
        name="fused",
    )(
        latent,
        context,
        conditioning,
        norm_gain.reshape(1, width),
        shift_weight,
        scale_weight,
        gate_weight,
        query_weight,
        key_weight,
        value_weight,
        out_weight,
        sink_logit,
    )


def solution(mesh):
    in_specs = (
        P(("grp", "sp", "tp"), None),
        P(("grp", "sp"), None),
        P(("grp", "sp")),
        P(),
        P("sp", "tp"),
        P("sp", "tp"),
        P("sp", "tp"),
        P(None, "tp"),
        P(None, "tp"),
        P(None, "tp"),
        P(None, "tp"),
        P("tp"),
    )
    out_specs = P(("grp", "sp", "tp"), None)
    return jax.shard_map(local, mesh=mesh, in_specs=in_specs, out_specs=out_specs, check_vma=False)
```

time: 66.7 us -> 66.2 us (level); the launches traced: 66.5 us -> 65.2 us
  other arithmetic: 2.51 us -> 0 us
  local copies, waits for them, and re-layouts: 0.01 us -> 2.29 us
  Pallas kernels: 64 us -> 62.9 us
    convert_element_type x1 -> x0, other arithmetic: 2.51 us -> none  [local(): return (latent.astype(f32) + gate * blended.astype(f32)).astype(bf16)]
    unnamed x2 -> x1, local copies, waits for them, and re-layouts: 0.01 us -> 2.29 us
    pallas_call x1, Pallas kernels: 64 us -> 62.9 us  [local(): pl.pallas_call(functools.partial(fused_kernel, sp), out_shape=jax.ShapeDt...]
where the time goes in v1:
time: 66.2 us; the launch traced here: 65.2 us
  Pallas kernels  62.9 us (95%)
  local copies, waits for them, and re-layouts  2.29 us (3%)
    pallas_call x1, Pallas kernels, local(): pl.pallas_call(functools.partial(fused_kernel, sp), out_shape=jax.ShapeDt...  62.9 us
    unnamed x1, local copies, waits for them, and re-layouts  2.29 us

profile of v1, /device:TPU:0, one launch (start us, length us, event | category | flops | bytes accessed | tf_op | source)
XLA Modules:
  0.0 65.2 jit_solution(8231989822663016515)
XLA Ops:
  0.0 62.9 %fused.1 = bf16[128,4096]{1,0:T(8,128)(2,1)} custom-call(bf16[128,4096]{1,0:T(8,128)(2,1)} %latent.1, bf16[192,4096]{1,0:T(8,128)(2,1)} %context.1, bf16[1024]{0:T(1024)(128)(2,1)} %conditioning.1, f32[1,4096]{1,0:T(1,128)} %bitcast.1, bf16[1024,1024]{1,0:T(8,128)(2,1)} %shift_weight.1, bf16[1024,1024]{1,0:T(8,128)(2,1)} %scale_weight.1, ...), custom_call_target="tpu_custom_call" | custom-call | tf_op jit(solution)/shard_map/fused/pallas_call | solution.py:934
  62.9 2.3 %copy.14 = bf16[128,4096]{1,0:T(8,128)(2,1)} copy(bf16[128,4096]{1,0:T(8,128)(2,1)} %fused.1) | data formatting | bytes 2097152

commit v2 on v1

--- a/solution.py
+++ b/solution.py
@@ -208,6 +208,7 @@
 WEIGHT_CHUNKS = 4
 AHEAD = 3
 NORM_ROWS = 16
+CONTEXT_ROWS = 32
 
 
 def remote(src, dst, send, recv, device):
@@ -241,6 +242,7 @@
     mod_w,
     proj_w,
     wo,
+    wo_shard,
     ctx_v,
     lat_own,
     lat_far,
@@ -262,8 +264,12 @@
     ctx_kv,
     att,
     att_out,
+    ctx_vt,
+    bias,
+    part_out,
+    part_top,
+    part_sum,
     out_part,
-    mixed_v,
     load_sem,
     lat_send,
     lat_recv,
@@ -320,14 +326,15 @@
 
     loads = [
         (latent, lat_own),
+        (out_weight.at[pl.ds(pl.multiple_of((g * sp + s) * shard, 16), shard)], wo_shard),
+        (norm_gain, gain_v),
+        (context, ctx_v),
+        (key_weight, proj_w.at[core, :, qw : qw + kw]),
+        (value_weight, proj_w.at[core, :, qw + kw : qw + 2 * kw]),
         (conditioning, cond_v),
         (shift_weight, mod_w.at[0]),
         (scale_weight, mod_w.at[1]),
         (gate_weight, mod_w.at[2]),
-        (norm_gain, gain_v),
-        (context, ctx_v),
-        (key_weight, proj_w.at[core, :, qw : qw + kw]),
-        (value_weight, proj_w.at[core, :, qw + kw : qw + 2 * kw]),
         (query_weight, proj_w.at[core, :, 0:qw]),
         (out_weight, wo.at[t]),
     ]
@@ -350,20 +357,27 @@
                     barrier, inc=1, device_id={**place, "tp": peer}, device_id_type=MESH
                 )
 
+    def row_factor(source, part):
+        squares = None
+        for at in range(0, width, 512):
+            values = source[part, at : at + 512].astype(f32)
+            values = values * values
+            squares = values if squares is None else squares + values
+        return lax.rsqrt(jnp.sum(squares, axis=-1, keepdims=True) * (1.0 / width) + epsilon)
+
     lane = lax.broadcasted_iota(jnp.int32, (rows, 128), 1)
     row = lax.broadcasted_iota(jnp.int32, (rows, 128), 0)
     diagonal = lane == row
 
     loads[0].wait()
+    loads[1].wait()
 
     def row_stat(i, carry):
-        part = pl.ds(pl.multiple_of(i * NORM_ROWS, NORM_ROWS), NORM_ROWS)
-        values = lat_own[part].astype(f32)
-        scale = lax.rsqrt(jnp.mean(values * values, axis=-1, keepdims=True) + epsilon)
-        row_scale[0, part] = jnp.broadcast_to(scale, (NORM_ROWS, 128))
+        part = pl.ds(pl.multiple_of(i * CONTEXT_ROWS, 16), CONTEXT_ROWS)
+        row_scale[0, part] = jnp.broadcast_to(row_factor(lat_own, part), (CONTEXT_ROWS, 128))
         return carry
 
-    lax.fori_loop(0, rows // NORM_ROWS, row_stat, 0)
+    lax.fori_loop(0, rows // CONTEXT_ROWS, row_stat, 0)
     flat = jnp.sum(jnp.where(diagonal, row_scale[0], 0.0), axis=0, keepdims=True)
     stat_out[...] = jnp.broadcast_to(flat, (8, 128))
     sink_row = lax.broadcasted_iota(jnp.int32, (8, 128), 0)
@@ -379,7 +393,7 @@
     def lat_copy(j):
         cols = pl.ds(pl.multiple_of(j * chunk, 128), chunk)
         return remote(
-            latent.at[:, cols], lat_far.at[:, cols], lat_send.at[j], lat_recv.at[j], far_dev
+            lat_own.at[:, cols], lat_far.at[:, cols], lat_send.at[j], lat_recv.at[j], far_dev
         )
 
     def wo_rows(gg, j, c):
@@ -388,14 +402,18 @@
     def wo_cross(c):
         part = wo_rows(g, s, c)
         return remote(
-            out_weight.at[part], wo.at[t, part], wox_send.at[c], wo_recv.at[s, c], far_dev
+            wo_shard.at[pl.ds(c * slab, slab)],
+            wo.at[t, part],
+            wox_send.at[c],
+            wo_recv.at[s, c],
+            far_dev,
         )
 
     stat_copy = remote(stat_out, stat_in, stat_sem.at[0], stat_sem.at[1], far_dev)
     stat_copy.start()
     for c in range(WEIGHT_CHUNKS):
         wo_cross(c).start()
-    for j in range(AHEAD):
+    for j in range(2):
         lat_copy(j).start()
     pair_copies = [
         (sink_v.at[core], sink_v.at[core]),
@@ -408,8 +426,7 @@
         remote(a, b, pair_send.at[i], pair_recv.at[i], pair_dev)
         for i, (a, b) in enumerate(pair_copies)
     ]
-    for copy in pair_copies:
-        copy.start()
+    pair_copies[0].start()
 
     def line_copy(at, j, send, recv, toward):
         return remote(at(j), at(j), send.at[toward, j], recv.at[j], (left_dev, right_dev)[toward])
@@ -449,7 +466,25 @@
     def ctx_at(j):
         return ctx_kv.at[core, pl.ds(pl.multiple_of(j * ctx_rows, 16), ctx_rows)]
 
-    for i in range(1, 5):
+    for i in range(2, 6):
+        loads[i].wait()
+
+    def norm_context(i, carry):
+        part = pl.ds(pl.multiple_of(i * CONTEXT_ROWS, 16), CONTEXT_ROWS)
+        scale = row_factor(ctx_v, part)
+        for at in range(0, width, 512):
+            here = slice(at, at + 512)
+            values = ctx_v[part, here].astype(f32)
+            ctx_v[part, here] = (values * scale * gain_v[:, here]).astype(bf16)
+        return carry
+
+    lax.fori_loop(0, ctx_rows // CONTEXT_ROWS, norm_context, 0)
+    own_ctx = pl.ds(pl.multiple_of(s * ctx_rows, 16), ctx_rows)
+    ctx_kv[core, own_ctx] = jnp.dot(
+        ctx_v[...], proj_w[core, :, qw : qw + 2 * kw], preferred_element_type=f32
+    ).astype(bf16)
+    line_start(ctx_at, ctxz_send, ctxz_recv)
+    for i in range(6, 10):
         loads[i].wait()
     cond = cond_v[...].astype(f32).reshape(1, cond_v.shape[0])
     lifted = jnp.broadcast_to(cond / (1.0 + jnp.exp(-cond)), (16, cond.shape[1])).astype(bf16)
@@ -458,24 +493,8 @@
             lifted, mod_w[i], preferred_element_type=f32
         )[0:1]
     line_start(mod_at, modz_send, modz_recv)
-
-    for i in range(5, 9):
-        loads[i].wait()
-
-    def norm_context(i, carry):
-        part = pl.ds(pl.multiple_of(i * NORM_ROWS, NORM_ROWS), NORM_ROWS)
-        values = ctx_v[part].astype(f32)
-        scale = lax.rsqrt(jnp.mean(values * values, axis=-1, keepdims=True) + epsilon)
-        ctx_v[part] = (values * scale * gain_v[...]).astype(bf16)
-        return carry
-
-    lax.fori_loop(0, ctx_rows // NORM_ROWS, norm_context, 0)
-    own_ctx = pl.ds(pl.multiple_of(s * ctx_rows, 16), ctx_rows)
-    ctx_kv[core, own_ctx] = jnp.dot(
-        ctx_v[...], proj_w[core, :, qw : qw + 2 * kw], preferred_element_type=f32
-    ).astype(bf16)
-    line_relay(1, mod_at, modz_send, modz_recv)
-    line_start(ctx_at, ctxz_send, ctxz_recv)
+    for copy in pair_copies[1:4]:
+        copy.start()
 
     def wo_line(j, c, toward):
         part = wo.at[far, wo_rows(g, j, c)]
@@ -485,17 +504,42 @@
 
     def wo_across(j, c):
         part = wo.at[far, wo_rows(g, j, c)]
-        return remote(part, part, woy_send, woy_recv, y_dev)
+        return remote(part, part, woy_send, woy_recv.at[j, c], y_dev)
+
+    def wo_share(j, c):
+        part = wo.at[far, wo_rows(1 - g, j, c)]
+        remote(part, part, woy_send, woy_recv.at[j, c], y_dev).wait_recv()
+        remote(part, part, wop_send.at[1 - g], wop_recv.at[1 - g], pair_dev).start()
+
+    def wo_shares(k):
+        def step(c, carry):
+            for j, there in ((s - k, s >= k), (s + k, s + k < sp)):
+
+                @pl.when(there)
+                def _():
+                    wo_share(j, c)
+
+            return carry
+
+        lax.fori_loop(0, WEIGHT_CHUNKS, step, 0)
+
+    def wo_share_own():
+        def step(c, carry):
+            wo_share(s, c)
+            return carry
+
+        lax.fori_loop(0, WEIGHT_CHUNKS, step, 0)
 
     def wo_own(c):
         wo_line(s, c, 0).wait_recv()
+        wo_across(s, c).start()
+
+    def wo_own_line(c):
         for toward, has in ((0, has_left), (1, has_right)):
 
             @pl.when(has)
             def _():
                 wo_line(s, c, toward).start()
-
-        wo_across(s, c).start()
 
     def wo_relay(e):
         k, c = e // WEIGHT_CHUNKS, lax.rem(e, WEIGHT_CHUNKS)
@@ -537,11 +581,39 @@
         turn_sin[b] = jnp.where(first, -sines, sines)
         return carry
 
+    contract = (((1,), (1,)), ((), ()))
+    band = 3 * rows
+    pairs = kw // HD
+    stack = group * rows
+
+    def biases(block, carry):
+        q_pos = lax.broadcasted_iota(jnp.int32, (band, rows), 1)
+        k_pos = lax.broadcasted_iota(jnp.int32, (band, rows), 0)
+        place = s * total + jnp.where(block == 0, t, far) * rows - WIN + k_pos
+        allowed = jnp.logical_and(
+            jnp.logical_and(k_pos >= q_pos, k_pos <= q_pos + 2 * WIN),
+            jnp.logical_and(place >= 0, place < sp * total),
+        )
+        bias[block] = jnp.where(allowed, 0.0, neg_large)
+        return carry
+
     wo_own(0)
+    wo_own_line(0)
+    line_relay(1, mod_at, modz_send, modz_recv)
+    line_relay(1, ctx_at, ctxz_send, ctxz_recv)
+    wo_own(1)
+    lax.fori_loop(0, 2, tables, 0)
+    lax.fori_loop(0, 2, biases, 0)
     line_relay(2, mod_at, modz_send, modz_recv)
-    lax.fori_loop(0, 2, tables, 0)
-    wo_own(1)
-    line_relay(1, ctx_at, ctxz_send, ctxz_recv)
+    for j in range(2, AHEAD):
+        lat_copy(j).start()
+    wo_own_line(1)
+    for c in range(2, WEIGHT_CHUNKS):
+        wo_own(c)
+        wo_own_line(c)
+    wo_relays(WEIGHT_CHUNKS, WEIGHT_CHUNKS + 1)
+    pair_copies[4].start()
+    line_relay(2, ctx_at, ctxz_send, ctxz_recv)
     for k in range(3, sp):
         line_relay(k, mod_at, modz_send, modz_recv)
     summed = mod_part[0]
@@ -559,15 +631,9 @@
         )
         copy.start()
         mods.append(copy)
-    for c in range(2, WEIGHT_CHUNKS):
-        wo_own(c)
-    line_relay(2, ctx_at, ctxz_send, ctxz_recv)
-    wo_relays(WEIGHT_CHUNKS, 2 * WEIGHT_CHUNKS)
-    for k in range(3, sp):
-        line_relay(k, ctx_at, ctxz_send, ctxz_recv)
-    ctx_pair = remote(ctx_kv.at[core], ctx_kv.at[core], ctxp_sem.at[0], ctxp_sem.at[1], pair_dev)
-    ctx_pair.start()
-
+    for j in range(AHEAD, LATENT_CHUNKS):
+        lat_copy(j).start()
+    wo_relays(WEIGHT_CHUNKS + 1, WEIGHT_CHUNKS + 3)
     stat_copy.wait_recv()
     column = jnp.sum(
         jnp.where(diagonal, jnp.broadcast_to(stat_in[0:1], (rows, 128)), 0.0), axis=1, keepdims=True
@@ -582,29 +648,20 @@
         factor_v[:, cols] = gain_v[:, cols] * (1.0 + mod_all[i, :, mod_cols : 2 * mod_cols])
         gate_v[:, cols] = mod_all[i, :, 2 * mod_cols : 3 * mod_cols]
 
-    def project(j, block, source):
+    def normalize(block, source, cols, lanes, target):
+        scale = row_scale[block]
+        for at in range(0, lanes, 128):
+            here = pl.ds(pl.multiple_of(cols + at, 128), 128)
+            values = source[:, here].astype(f32) * scale
+            target[:, at : at + 128] = (values * factor_v[:, here] + shift_v[:, here]).astype(bf16)
+
+    def project(j):
+        normalize(1, lat_far, j * chunk, chunk, normed)
         cols = pl.ds(pl.multiple_of(j * chunk, 128), chunk)
-
-        def norm_rows(i, carry):
-            part = pl.ds(pl.multiple_of(i * NORM_ROWS, NORM_ROWS), NORM_ROWS)
-            values = source[part, cols].astype(f32)
-            scale = row_scale[block, part, 0:1]
-            normed[part] = (values * scale * factor_v[:, cols] + shift_v[:, cols]).astype(bf16)
-            return carry
-
-        lax.fori_loop(0, rows // NORM_ROWS, norm_rows, 0)
         for slot in range(2):
-            product = jnp.dot(
-                normed[...], proj_w[slot, cols], preferred_element_type=f32
+            acc[slot] += jnp.dot(
+                normed[:, 0:chunk], proj_w[slot, cols], preferred_element_type=f32
             )
-
-            @pl.when(j == 0)
-            def _():
-                acc[slot] = product
-
-            @pl.when(j != 0)
-            def _():
-                acc[slot] = acc[slot] + product
 
     low = lane < HD
 
@@ -622,18 +679,16 @@
         for slot in range(2):
             key_value[slot, base, 0:kw] = turned(acc[slot, :, qw : qw + kw]).astype(bf16)
             key_value[slot, base, kw : 2 * kw] = acc[slot, :, qw + kw : qw + 2 * kw].astype(bf16)
-            for h in range(heads):
-                lanes = acc[slot, :, (h // 2) * 128 : (h // 2 + 1) * 128]
-                lanes = turned(lanes).astype(bf16).astype(f32) * factor
-                at, want = h % 2, h // group
-                if at != want:
-                    lanes = pltpu.roll(lanes, HD, 1)
-                keep = low if want == 0 else jnp.logical_not(low)
-                lanes = jnp.where(keep, lanes, 0.0).astype(bf16)
-                for n in range(2):
-                    queries[block, n, slot, h * half : (h + 1) * half] = lanes[
-                        n * half : (n + 1) * half
-                    ]
+            for u in range(heads // 2):
+                lanes = turned(acc[slot, :, u * 128 : (u + 1) * 128]).astype(bf16)
+                swapped = pltpu.roll(lanes.astype(f32), HD, 1) * factor
+                lanes = lanes.astype(f32) * factor
+                keep = low if u == 0 else jnp.logical_not(low)
+                for at in range(2):
+                    aligned = lanes if at == u else swapped
+                    queries[block, slot, u, at * rows : (at + 1) * rows] = jnp.where(
+                        keep, aligned, 0.0
+                    ).astype(bf16)
 
     def kv_at(position):
         return key_value.at[:, pl.ds(pl.multiple_of(position * rows, rows), rows)]
@@ -668,6 +723,76 @@
         def _():
             halo_down.wait_recv()
 
+    def context_part(block, slot):
+        units = range(pairs)
+        scores = [
+            lax.dot_general(
+                ctx_kv[slot, :, 0:kw],
+                queries[block, slot, u],
+                contract,
+                preferred_element_type=f32,
+            )
+            for u in units
+        ]
+        sinks = [
+            jnp.concatenate(
+                [sink_v[slot, u * group + h : u * group + h + 1] for h in range(group)], axis=1
+            )
+            for u in units
+        ]
+        tops = [
+            jnp.maximum(jnp.max(scores[u], axis=0, keepdims=True), sinks[u]) for u in units
+        ]
+        exps = [jnp.exp(scores[u] - tops[u]) for u in units]
+        for u in units:
+            part_top[block, slot, u] = tops[u]
+            part_sum[block, slot, u] = jnp.sum(exps[u], axis=0, keepdims=True) + jnp.exp(
+                sinks[u] - tops[u]
+            )
+            part_out[block, slot, u] = jnp.dot(
+                ctx_vt[slot, u * HD : (u + 1) * HD],
+                exps[u].astype(bf16),
+                preferred_element_type=f32,
+            )
+
+    def window_part(block, position, slot, target):
+        units = range(pairs)
+        window = pl.ds(pl.multiple_of((position - 1) * rows, rows), band)
+        mask = jnp.concatenate([bias[block]] * group, axis=1)
+        scores = [
+            lax.dot_general(
+                key_value[slot, window, 0:kw],
+                queries[block, slot, u],
+                contract,
+                preferred_element_type=f32,
+            )
+            + mask
+            for u in units
+        ]
+        befores = [part_top[block, slot, u] for u in units]
+        tops = [
+            jnp.maximum(jnp.max(scores[u], axis=0, keepdims=True), befores[u]) for u in units
+        ]
+        exps = [jnp.exp(scores[u] - tops[u]) for u in units]
+        keeps = [jnp.exp(befores[u] - tops[u]) for u in units]
+        values = jnp.transpose(key_value[slot, window, kw : 2 * kw])
+        for u in units:
+            bottom = (
+                jnp.sum(exps[u], axis=0, keepdims=True) + part_sum[block, slot, u] * keeps[u]
+            )
+            result = (
+                jnp.dot(
+                    values[u * HD : (u + 1) * HD],
+                    exps[u].astype(bf16),
+                    preferred_element_type=f32,
+                )
+                + part_out[block, slot, u] * keeps[u]
+            ) / bottom
+            turned_back = jnp.concatenate(
+                [result[:, h * rows : (h + 1) * rows] for h in range(group)], axis=0
+            )
+            target[slot, :, u * 128 : (u + 1) * 128] = jnp.transpose(turned_back).astype(bf16)
+
     edge = jnp.zeros((2, rows, 2 * kw), bf16)
 
     @pl.when(jnp.logical_and(core == 0, jnp.logical_not(has_left)))
@@ -678,130 +803,90 @@
     def _():
         key_value[:, (tp + 1) * rows : (tp + 2) * rows] = edge
 
-    for i in range(9, 11):
+    for i in range(10, 12):
         loads[i].wait()
     for copy in pair_copies[0:4]:
         copy.wait_recv()
 
-    def own_step(j, carry):
-        project(j, 0, lat_own)
+    def far_step(j, carry):
+        lat_copy(j).wait_recv()
+        project(j)
         return carry
 
-    lax.fori_loop(0, LATENT_CHUNKS, own_step, 0)
+    normalize(0, lat_own, 0, width, normed)
+    for slot in range(2):
+        acc[slot] = jnp.dot(normed[...], proj_w[slot], preferred_element_type=f32)
     finish_projection(0, t + 1)
     kv_pair(0, t + 1).start()
     send_halo(chip == core)
-
-    def far_step(j, carry):
-        @pl.when(j < 4)
-        def _():
-            wo_relays(2 * WEIGHT_CHUNKS + 2 * j, 2 * WEIGHT_CHUNKS + 2 * j + 2)
-
-        lat_copy(j).wait_recv()
-
-        @pl.when(j + AHEAD < LATENT_CHUNKS)
-        def _():
-            lat_copy(j + AHEAD).start()
-
-        project(j, 1, lat_far)
-        return carry
-
-    lax.fori_loop(0, LATENT_CHUNKS, far_step, 0)
+    def wo_pair(gg):
+        part = wo.at[far, pl.ds(pl.multiple_of(gg * sp * shard, 16), sp * shard)]
+        return remote(part, part, wop_send.at[gg], wop_recv.at[gg], pair_dev)
+
+
+    def wo_last(c):
+        for k in range(3, sp):
+            wo_relays(k * WEIGHT_CHUNKS + c, k * WEIGHT_CHUNKS + c + 1)
+
+    wo_relays(WEIGHT_CHUNKS + 3, 2 * WEIGHT_CHUNKS + 1)
+    for slot in range(2):
+        acc[slot] = jnp.zeros(acc.shape[1:], f32)
+    lax.fori_loop(0, 3, far_step, 0)
+    wo_relays(2 * WEIGHT_CHUNKS + 1, 3 * WEIGHT_CHUNKS)
+    for k in range(3, sp):
+        line_relay(k, ctx_at, ctxz_send, ctxz_recv)
+    ctx_pair = remote(ctx_kv.at[core], ctx_kv.at[core], ctxp_sem.at[0], ctxp_sem.at[1], pair_dev)
+    ctx_pair.start()
+    lax.fori_loop(3, 5, far_step, 0)
+    ctx_pair.wait_recv()
+    for slot in range(2):
+        ctx_vt[slot] = jnp.transpose(ctx_kv[slot, :, kw : 2 * kw])
+
+    for slot in range(2):
+        context_part(0, slot)
+    wo_last(0)
+    lax.fori_loop(5, 6, far_step, 0)
+    wo_last(1)
+    lax.fori_loop(6, 7, far_step, 0)
+    wo_last(2)
+    lax.fori_loop(7, LATENT_CHUNKS, far_step, 0)
     finish_projection(1, far + 1)
     kv_pair(1, far + 1).start()
     send_halo(chip != core)
 
-    def wo_pair(gg):
-        part = wo.at[far, pl.ds(pl.multiple_of(gg * sp * shard, 16), sp * shard)]
-        return remote(part, part, wop_send.at[gg], wop_recv.at[gg], pair_dev)
-
+    for c in range(3, WEIGHT_CHUNKS):
+        wo_last(c)
     wo_pair(g).start()
-
+    for slot in range(2):
+        context_part(1, slot)
+    wo_share_own()
+    wo_shares(1)
     kv_pair(0, pair + 1).wait_recv()
-    ctx_pair.wait_recv()
-
-    contract = (((1,), (1,)), ((), ()))
-    band = 2 * WIN + half
-    stack = heads * half
-    q_pos = lax.rem(lax.broadcasted_iota(jnp.int32, (stack, band), 0), half)
-    k_pos = lax.broadcasted_iota(jnp.int32, (stack, band), 1)
-    in_window = jnp.logical_and(k_pos >= q_pos, k_pos <= q_pos + 2 * WIN)
-
-    def attend(block, position, n, slot, target):
-        start = pl.multiple_of((position - 1) * rows + n * half, half)
-        band_k = key_value[slot, pl.ds(start, band), 0:kw]
-        band_v = key_value[slot, pl.ds(start, band), kw : 2 * kw]
-        ctx_k = ctx_kv[slot, :, 0:kw]
-        ctx_v_ = ctx_kv[slot, :, kw : 2 * kw]
-        sinks = jnp.concatenate(
-            [jnp.broadcast_to(sink_v[slot, h : h + 1, 0:1], (half, 1)) for h in range(heads)],
-            axis=0,
-        )
-        place = s * total + start - WIN + k_pos
-        allowed = jnp.logical_and(in_window, jnp.logical_and(place >= 0, place < sp * total))
-        q = queries[block, n, slot]
-        near_s = lax.dot_general(q, band_k, contract, preferred_element_type=f32)
-        near_s = jnp.where(allowed, near_s, neg_large)
-        ctx_s = lax.dot_general(q, ctx_k, contract, preferred_element_type=f32)
-        top = jnp.maximum(
-            jnp.max(near_s, axis=-1, keepdims=True), jnp.max(ctx_s, axis=-1, keepdims=True)
-        )
-        top = jnp.maximum(top, sinks)
-        near_e = jnp.exp(near_s - top)
-        ctx_e = jnp.exp(ctx_s - top)
-        bottom = (
-            jnp.sum(near_e, axis=-1, keepdims=True)
-            + jnp.sum(ctx_e, axis=-1, keepdims=True)
-            + jnp.exp(sinks - top)
-        )
-        share = 1.0 / bottom
-        result = jnp.dot(
-            (near_e * share).astype(bf16), band_v, preferred_element_type=f32
-        ) + jnp.dot((ctx_e * share).astype(bf16), ctx_v_, preferred_element_type=f32)
-        for v in range(qw // 128):
-            sides = []
-            for at in range(2):
-                h = 2 * v + at
-                lanes = result[h * half : (h + 1) * half]
-                if h // group != at:
-                    lanes = pltpu.roll(lanes, HD, 1)
-                sides.append(lanes)
-            target[
-                slot, pl.ds(pl.multiple_of(n * half, half), half), v * 128 : (v + 1) * 128
-            ] = jnp.where(low[:half], sides[0], sides[1]).astype(bf16)
-
-    def att_copy(n):
-        part = pl.ds(pl.multiple_of(n * half, half), half)
+
+    def att_copy(slot):
         return remote(
-            att_out.at[:, part], att.at[chip, :, part], att_send.at[n], att_recv.at[n], far_dev
+            att_out.at[slot], att.at[chip, slot], att_send.at[slot], att_recv.at[slot], far_dev
         )
 
     kv_pair(1, pair + 1).wait_recv()
     wait_halo(chip != core)
 
-    def far_attend(i, carry):
-        n, slot = i // 2, lax.rem(i, 2)
-        attend(1, far + 1, n, slot, att_out)
-
-        @pl.when(slot == 1)
-        def _():
-            att_copy(n).start()
-
+    def far_attend(n, carry):
+        window_part(1, far + 1, n, att_out)
+        att_copy(n).start()
         return carry
 
-    lax.fori_loop(0, 4, far_attend, 0)
-    wo_gathered = wo.at[far, pl.ds(pl.multiple_of((1 - g) * sp * shard, 16), sp * shard)]
-    remote(wo_gathered, wo_gathered, woy_send, woy_recv, y_dev).wait_recv()
-    wo_pair(1 - g).start()
+    lax.fori_loop(0, 2, far_attend, 0)
+    wo_shares(2)
     wait_halo(chip == core)
 
-    def own_attend(i, carry):
-        n, slot = i // 2, lax.rem(i, 2)
-        attend(0, t + 1, n, slot, att.at[chip])
+    def own_attend(n, carry):
+        window_part(0, t + 1, n, att.at[chip])
         return carry
 
-    lax.fori_loop(0, 4, own_attend, 0)
-
+    lax.fori_loop(0, 2, own_attend, 0)
+    for k in range(3, sp):
+        wo_shares(k)
     pair_copies[4].wait_recv()
 
     def out_product(x, i):
@@ -822,16 +907,10 @@
         out_part[k] = out_product(chip, i)
     att_copy(0).wait_recv()
     att_copy(1).wait_recv()
-    stores = []
     for k, i in enumerate(order):
         cols = pl.ds(pl.multiple_of(i * out_width, 128), out_width)
         blended = (out_part[k] + out_product(1 - chip, i)).astype(bf16).astype(f32)
-        mixed_v[:, cols] = (lat_own[:, cols].astype(f32) + gate_v[:, cols] * blended).astype(bf16)
-        store = pltpu.make_async_copy(
-            mixed_v.at[:, cols], mixed.at[:, cols], load_sem.at[len(loads) + k]
-        )
-        store.start()
-        stores.append(store)
+        mixed[:, cols] = (lat_own[:, cols].astype(f32) + gate_v[:, cols] * blended).astype(bf16)
 
     stat_copy.wait_send()
     for c in range(WEIGHT_CHUNKS):
@@ -857,7 +936,7 @@
                 lax.fori_loop(0, WEIGHT_CHUNKS, step, 0)
 
     wo_sent = wo.at[far, pl.ds(pl.multiple_of(g * sp * shard, 16), sp * shard)]
-    remote(wo_sent, wo_sent, woy_send, woy_recv, y_dev).wait_send()
+    remote(wo_sent, wo_sent, woy_send, woy_recv.at[0, 0], y_dev).wait_send()
     wo_pair(0).wait_send()
     wo_pair(1).wait_send()
     kv_pair(0, t + 1).wait_send()
@@ -873,8 +952,6 @@
 
     att_copy(0).wait_send()
     att_copy(1).wait_send()
-    for store in stores:
-        store.wait()
 
 
 def local(
@@ -905,7 +982,9 @@
         and tp == 4
         and grp == 2
         and sp >= 3
-        and ctx_rows % NORM_ROWS == 0
+        and sp * ctx_rows % 128 == 0
+        and ctx_rows % CONTEXT_ROWS == 0
+        and width % 512 == 0
         and mod_cols % 128 == 0
         and width % (128 * LATENT_CHUNKS) == 0
         and out_width % 128 == 0
@@ -933,19 +1012,20 @@
     anywhere = pl.BlockSpec(memory_space=pl.ANY)
     return pl.pallas_call(
         functools.partial(fused_kernel, sp),
-        out_shape=jax.ShapeDtypeStruct((rows, width), bf16),
+        out_shape=pltpu.VMEM((rows, width), bf16),
         in_specs=[anywhere] * 11 + [pl.BlockSpec(memory_space=pltpu.SMEM)],
-        out_specs=anywhere,
+        out_specs=pl.BlockSpec(memory_space=pltpu.VMEM),
         scratch_shapes=[
             pltpu.VMEM((mod_rows,), bf16),
             pltpu.VMEM((1, width), f32),
             pltpu.VMEM((3, mod_rows, mod_cols), bf16),
             pltpu.VMEM((2, width, query_width + 2 * key_width), bf16),
             pltpu.VMEM((tp, out_rows, out_width), bf16),
+            pltpu.VMEM((out_rows // (2 * sp), out_width), bf16),
             pltpu.VMEM(context.shape, bf16),
             pltpu.VMEM((rows, width), bf16),
             pltpu.VMEM((rows, width), bf16),
-            pltpu.VMEM((rows, width // LATENT_CHUNKS), bf16),
+            pltpu.VMEM((rows, width), bf16),
             pltpu.VMEM((8, 128), f32),
             pltpu.VMEM((8, 128), f32),
             pltpu.VMEM((2, rows, 128), f32),
@@ -958,14 +1038,18 @@
             pltpu.VMEM((2, rows, 128), f32),
             pltpu.VMEM((2, rows, 128), f32),
             pltpu.VMEM((2, rows, query_width + 2 * key_width), f32),
-            pltpu.VMEM((2, 2, 2, query_width // HD * (rows // 2), key_width), bf16),
+            pltpu.VMEM((2, 2, 2, 2 * rows, key_width), bf16),
             pltpu.VMEM((2, (tp + 2) * rows, 2 * key_width), bf16),
             pltpu.VMEM((2, sp * ctx_rows, 2 * key_width), bf16),
             pltpu.VMEM((2, 2, rows, query_width), bf16),
             pltpu.VMEM((2, rows, query_width), bf16),
+            pltpu.VMEM((2, key_width, sp * ctx_rows), bf16),
+            pltpu.VMEM((2, 3 * rows, rows), f32),
+            pltpu.VMEM((2, 2, 2, HD, 2 * rows), f32),
+            pltpu.VMEM((2, 2, 2, 1, 2 * rows), f32),
+            pltpu.VMEM((2, 2, 2, 1, 2 * rows), f32),
             pltpu.VMEM((tp, rows, out_width), f32),
-            pltpu.VMEM((rows, width), bf16),
-            dma((15,)),
+            dma((12,)),
             dma((LATENT_CHUNKS,)),
             dma((LATENT_CHUNKS,)),
             dma((2,)),
@@ -975,7 +1059,7 @@
             dma((2, sp, WEIGHT_CHUNKS)),
             dma((sp, WEIGHT_CHUNKS)),
             dma,
-            dma,
+            dma((sp, WEIGHT_CHUNKS)),
             dma((2,)),
             dma((2,)),
             dma((2, sp)),

time: 66.2 us -> 47.5 us (0.72); the launches traced: 65.2 us -> 47.4 us
  Pallas kernels: 62.9 us -> 46.4 us
  local copies, waits for them, and re-layouts: 2.29 us -> 0.97 us
    pallas_call x1, Pallas kernels: 62.9 us -> 46.4 us  [local(): pl.pallas_call(functools.partial(fused_kernel, sp), out_shape=pltpu.VMEM(...]
    unnamed x1, local copies, waits for them, and re-layouts: 2.29 us -> 0.97 us
where the time goes in v2:
time: 47.5 us; the launch traced here: 47.4 us
  Pallas kernels  46.4 us (98%)
  local copies, waits for them, and re-layouts  0.97 us (2%)
    pallas_call x1, Pallas kernels, local(): pl.pallas_call(functools.partial(fused_kernel, sp), out_shape=pltpu.VMEM(...  46.4 us
    unnamed x1, local copies, waits for them, and re-layouts  0.97 us

profile of v2, /device:TPU:0, one launch (start us, length us, event | category | flops | bytes accessed | tf_op | source)
XLA Modules:
  0.0 47.4 jit_solution(17316533640053425661)
XLA Ops:
  0.0 46.4 %fused.1 = bf16[128,4096]{1,0:T(8,128)(2,1)S(1)} custom-call(bf16[128,4096]{1,0:T(8,128)(2,1)} %latent.1, bf16[192,4096]{1,0:T(8,128)(2,1)} %context.1, bf16[1024]{0:T(1024)(128)(2,1)} %conditioning.1, f32[1,4096]{1,0:T(1,128)} %bitcast.1, bf16[1024,1024]{1,0:T(8,128)(2,1)} %shift_weight.1, bf16[1024,1024]{1,0:T(8,128)(2,1)} %scale_weight.1, ...), custom_call_target="tpu_custom_call" | custom-call | tf_op jit(solution)/shard_map/fused/pallas_call | solution.py:1013
  46.4 1.0 %copy.14 = bf16[128,4096]{1,0:T(8,128)(2,1)} copy(bf16[128,4096]{1,0:T(8,128)(2,1)S(1)} %fused.1) | data formatting | bytes 2097152

commit v3 on v2

--- a/solution.py
+++ b/solution.py
@@ -325,8 +325,8 @@
     MESH = pl.DeviceIdType.MESH
 
     loads = [
+        (out_weight.at[pl.ds(pl.multiple_of((g * sp + s) * shard, 16), shard)], wo_shard),
         (latent, lat_own),
-        (out_weight.at[pl.ds(pl.multiple_of((g * sp + s) * shard, 16), shard)], wo_shard),
         (norm_gain, gain_v),
         (context, ctx_v),
         (key_weight, proj_w.at[core, :, qw : qw + kw]),
@@ -369,7 +369,32 @@
     row = lax.broadcasted_iota(jnp.int32, (rows, 128), 0)
     diagonal = lane == row
 
+    pl.semaphore_wait(
+        barrier, tp + jnp.where(has_right, 2, 0) + jnp.where(has_left, 2, 0)
+    )
+
+    def lat_copy(j):
+        cols = pl.ds(pl.multiple_of(j * chunk, 128), chunk)
+        return remote(
+            lat_own.at[:, cols], lat_far.at[:, cols], lat_send, lat_recv.at[j], far_dev
+        )
+
+    def wo_rows(gg, j, c):
+        return pl.ds(pl.multiple_of((gg * sp + j) * shard + c * slab, 16), slab)
+
+    def wo_cross(c):
+        part = wo_rows(g, s, c)
+        return remote(
+            wo_shard.at[pl.ds(c * slab, slab)],
+            wo.at[t, part],
+            wox_send,
+            wo_recv.at[s, c],
+            far_dev,
+        )
+
     loads[0].wait()
+    for c in range(WEIGHT_CHUNKS):
+        wo_cross(c).start()
     loads[1].wait()
 
     def row_stat(i, carry):
@@ -386,33 +411,8 @@
         sink_all = jnp.where(sink_row == h, sink[h], sink_all)
     sink_v[core] = sink_all
 
-    pl.semaphore_wait(
-        barrier, tp + jnp.where(has_right, 2, 0) + jnp.where(has_left, 2, 0)
-    )
-
-    def lat_copy(j):
-        cols = pl.ds(pl.multiple_of(j * chunk, 128), chunk)
-        return remote(
-            lat_own.at[:, cols], lat_far.at[:, cols], lat_send.at[j], lat_recv.at[j], far_dev
-        )
-
-    def wo_rows(gg, j, c):
-        return pl.ds(pl.multiple_of((gg * sp + j) * shard + c * slab, 16), slab)
-
-    def wo_cross(c):
-        part = wo_rows(g, s, c)
-        return remote(
-            wo_shard.at[pl.ds(c * slab, slab)],
-            wo.at[t, part],
-            wox_send.at[c],
-            wo_recv.at[s, c],
-            far_dev,
-        )
-
     stat_copy = remote(stat_out, stat_in, stat_sem.at[0], stat_sem.at[1], far_dev)
     stat_copy.start()
-    for c in range(WEIGHT_CHUNKS):
-        wo_cross(c).start()
     for j in range(2):
         lat_copy(j).start()
     pair_copies = [
@@ -429,7 +429,7 @@
     pair_copies[0].start()
 
     def line_copy(at, j, send, recv, toward):
-        return remote(at(j), at(j), send.at[toward, j], recv.at[j], (left_dev, right_dev)[toward])
+        return remote(at(j), at(j), send.at[toward], recv.at[j], (left_dev, right_dev)[toward])
 
     def line_start(at, send, recv):
         for toward, has in ((0, has_left), (1, has_right)):
@@ -452,13 +452,14 @@
                 def _():
                     line_copy(at, j, send, recv, toward).start()
 
-    def line_finish(at, send, recv):
-        for j in range(sp):
-            for toward, has, sent in ((1, has_right, j <= s), (0, has_left, j >= s)):
-
-                @pl.when(jnp.logical_and(has, sent))
+    def line_finish(total_of, send):
+        for toward, has, sent in ((1, has_right, s + 1), (0, has_left, sp - s)):
+            for count in range(1, sp + 1):
+
+                @pl.when(jnp.logical_and(has, sent == count))
                 def _():
-                    line_copy(at, j, send, recv, toward).wait_send()
+                    part = total_of(count)
+                    remote(part, part, send.at[toward], stat_sem.at[1], right_dev).wait_send()
 
     def mod_at(j):
         return mod_part.at[j]
@@ -499,12 +500,16 @@
     def wo_line(j, c, toward):
         part = wo.at[far, wo_rows(g, j, c)]
         return remote(
-            part, part, wo_send.at[toward, j, c], wo_recv.at[j, c], (left_dev, right_dev)[toward]
+            part, part, wo_send.at[toward], wo_recv.at[j, c], (left_dev, right_dev)[toward]
         )
 
     def wo_across(j, c):
         part = wo.at[far, wo_rows(g, j, c)]
         return remote(part, part, woy_send, woy_recv.at[j, c], y_dev)
+
+    def wo_pass(j, c):
+        part = wo.at[far, wo_rows(g, j, c)]
+        remote(part, part, wop_send.at[g], wop_recv.at[g], pair_dev).start()
 
     def wo_share(j, c):
         part = wo.at[far, wo_rows(1 - g, j, c)]
@@ -533,6 +538,7 @@
     def wo_own(c):
         wo_line(s, c, 0).wait_recv()
         wo_across(s, c).start()
+        wo_pass(s, c)
 
     def wo_own_line(c):
         for toward, has in ((0, has_left), (1, has_right)):
@@ -557,6 +563,7 @@
                     wo_line(j, c, toward).start()
 
                 wo_across(j, c).start()
+                wo_pass(j, c)
 
     def wo_relays(low, high):
         def step(e, carry):
@@ -620,17 +627,13 @@
     for k in range(1, sp):
         summed = summed + mod_part[k]
     mod_all[t] = summed
-    mods = []
     for k in range(1, tp):
-        copy = remote(
-            mod_all.at[t],
-            mod_all.at[t],
-            modt_send.at[k - 1],
-            modt_recv.at[k - 1],
-            {"tp": lax.rem(t + k, tp)},
-        )
-        copy.start()
-        mods.append(copy)
+        remote(
+            mod_all.at[t], mod_all.at[t], modt_send, modt_recv, {"tp": lax.rem(t + k, tp)}
+        ).start()
+    mods = remote(
+        mod_all.at[0 : tp - 1], mod_all.at[0 : tp - 1], modt_send, modt_recv, pair_dev
+    )
     for j in range(AHEAD, LATENT_CHUNKS):
         lat_copy(j).start()
     wo_relays(WEIGHT_CHUNKS + 1, WEIGHT_CHUNKS + 3)
@@ -640,8 +643,7 @@
     )
     row_scale[1] = jnp.broadcast_to(column, (rows, 128))
 
-    for copy in mods:
-        copy.wait_recv()
+    mods.wait_recv()
     for i in range(tp):
         cols = slice(i * mod_cols, (i + 1) * mod_cols)
         shift_v[:, cols] = mod_all[i, :, 0:mod_cols]
@@ -695,7 +697,7 @@
 
     def kv_pair(block, position):
         return remote(
-            kv_at(position), kv_at(position), kv_send.at[block], kv_recv.at[block], pair_dev
+            kv_at(position), kv_at(position), kv_send, kv_recv.at[block], pair_dev
         )
 
     halo_down = remote(
@@ -755,10 +757,11 @@
                 preferred_element_type=f32,
             )
 
-    def window_part(block, position, slot, target):
+    def window_part(block, position, slot, skip, blocks):
         units = range(pairs)
-        window = pl.ds(pl.multiple_of((position - 1) * rows, rows), band)
-        mask = jnp.concatenate([bias[block]] * group, axis=1)
+        here = pl.ds(pl.multiple_of(skip * rows, rows), blocks * rows)
+        window = pl.ds(pl.multiple_of((position - 1 + skip) * rows, rows), blocks * rows)
+        mask = jnp.concatenate([bias[block, here]] * group, axis=1)
         scores = [
             lax.dot_general(
                 key_value[slot, window, 0:kw],
@@ -776,18 +779,30 @@
         exps = [jnp.exp(scores[u] - tops[u]) for u in units]
         keeps = [jnp.exp(befores[u] - tops[u]) for u in units]
         values = jnp.transpose(key_value[slot, window, kw : 2 * kw])
-        for u in units:
-            bottom = (
-                jnp.sum(exps[u], axis=0, keepdims=True) + part_sum[block, slot, u] * keeps[u]
+        bottoms = [
+            jnp.sum(exps[u], axis=0, keepdims=True) + part_sum[block, slot, u] * keeps[u]
+            for u in units
+        ]
+        results = [
+            jnp.dot(
+                values[u * HD : (u + 1) * HD], exps[u].astype(bf16), preferred_element_type=f32
             )
-            result = (
-                jnp.dot(
-                    values[u * HD : (u + 1) * HD],
-                    exps[u].astype(bf16),
-                    preferred_element_type=f32,
-                )
-                + part_out[block, slot, u] * keeps[u]
-            ) / bottom
+            + part_out[block, slot, u] * keeps[u]
+            for u in units
+        ]
+        return tops, bottoms, results
+
+    def window_early(block, position, slot, skip, blocks):
+        tops, bottoms, results = window_part(block, position, slot, skip, blocks)
+        for u in range(pairs):
+            part_top[block, slot, u] = tops[u]
+            part_sum[block, slot, u] = bottoms[u]
+            part_out[block, slot, u] = results[u]
+
+    def window_last(block, position, slot, skip, blocks, target):
+        _, bottoms, results = window_part(block, position, slot, skip, blocks)
+        for u in range(pairs):
+            result = results[u] / bottoms[u]
             turned_back = jnp.concatenate(
                 [result[:, h * rows : (h + 1) * rows] for h in range(group)], axis=0
             )
@@ -832,59 +847,54 @@
     for slot in range(2):
         acc[slot] = jnp.zeros(acc.shape[1:], f32)
     lax.fori_loop(0, 3, far_step, 0)
-    wo_relays(2 * WEIGHT_CHUNKS + 1, 3 * WEIGHT_CHUNKS)
     for k in range(3, sp):
         line_relay(k, ctx_at, ctxz_send, ctxz_recv)
     ctx_pair = remote(ctx_kv.at[core], ctx_kv.at[core], ctxp_sem.at[0], ctxp_sem.at[1], pair_dev)
     ctx_pair.start()
+    wo_relays(2 * WEIGHT_CHUNKS + 1, 2 * WEIGHT_CHUNKS + 2)
     lax.fori_loop(3, 5, far_step, 0)
+    wo_relays(2 * WEIGHT_CHUNKS + 2, 2 * WEIGHT_CHUNKS + 3)
     ctx_pair.wait_recv()
     for slot in range(2):
         ctx_vt[slot] = jnp.transpose(ctx_kv[slot, :, kw : 2 * kw])
-
-    for slot in range(2):
-        context_part(0, slot)
+    context_part(0, 0)
+    kv_pair(0, pair + 1).wait_recv()
+    window_early(0, t + 1, 0, 1 - core, 2)
+    wo_relays(2 * WEIGHT_CHUNKS + 3, 3 * WEIGHT_CHUNKS)
+    context_part(0, 1)
+    window_early(0, t + 1, 1, 1 - core, 2)
     wo_last(0)
+    wo_share_own()
+    wo_shares(1)
     lax.fori_loop(5, 6, far_step, 0)
     wo_last(1)
     lax.fori_loop(6, 7, far_step, 0)
     wo_last(2)
     lax.fori_loop(7, LATENT_CHUNKS, far_step, 0)
+    for c in range(3, WEIGHT_CHUNKS):
+        wo_last(c)
     finish_projection(1, far + 1)
     kv_pair(1, far + 1).start()
     send_halo(chip != core)
 
-    for c in range(3, WEIGHT_CHUNKS):
-        wo_last(c)
-    wo_pair(g).start()
-    for slot in range(2):
-        context_part(1, slot)
-    wo_share_own()
-    wo_shares(1)
-    kv_pair(0, pair + 1).wait_recv()
+    context_part(1, 0)
 
     def att_copy(slot):
         return remote(
-            att_out.at[slot], att.at[chip, slot], att_send.at[slot], att_recv.at[slot], far_dev
+            att_out.at[slot], att.at[chip, slot], att_send, att_recv.at[slot], far_dev
         )
 
     kv_pair(1, pair + 1).wait_recv()
     wait_halo(chip != core)
-
-    def far_attend(n, carry):
-        window_part(1, far + 1, n, att_out)
-        att_copy(n).start()
-        return carry
-
-    lax.fori_loop(0, 2, far_attend, 0)
+    window_last(1, far + 1, 0, 0, 3, att_out)
+    att_copy(0).start()
+    context_part(1, 1)
+    window_last(1, far + 1, 1, 0, 3, att_out)
+    att_copy(1).start()
     wo_shares(2)
     wait_halo(chip == core)
-
-    def own_attend(n, carry):
-        window_part(0, t + 1, n, att.at[chip])
-        return carry
-
-    lax.fori_loop(0, 2, own_attend, 0)
+    for slot in range(2):
+        window_last(0, t + 1, slot, 2 * core, 1, att.at[chip])
     for k in range(3, sp):
         wo_shares(k)
     pair_copies[4].wait_recv()
@@ -906,41 +916,38 @@
                 remote(part, part, wop_send.at[gg], wop_recv.at[gg], pair_dev).wait_recv()
         out_part[k] = out_product(chip, i)
     att_copy(0).wait_recv()
+    first_rows = pl.ds(pl.multiple_of(2 * (1 - chip) * qw, qw), qw)
+    last_rows = pl.ds(pl.multiple_of((2 * (1 - chip) + 1) * qw, qw), qw)
+    for k, i in enumerate(order):
+        out_part[k] += jnp.dot(
+            att[1 - chip, 0], wo[i, first_rows], preferred_element_type=f32
+        )
     att_copy(1).wait_recv()
     for k, i in enumerate(order):
         cols = pl.ds(pl.multiple_of(i * out_width, 128), out_width)
-        blended = (out_part[k] + out_product(1 - chip, i)).astype(bf16).astype(f32)
+        product = jnp.dot(att[1 - chip, 1], wo[i, last_rows], preferred_element_type=f32)
+        blended = (out_part[k] + product).astype(bf16).astype(f32)
         mixed[:, cols] = (lat_own[:, cols].astype(f32) + gate_v[:, cols] * blended).astype(bf16)
 
     stat_copy.wait_send()
-    for c in range(WEIGHT_CHUNKS):
-        wo_cross(c).wait_send()
-    for j in range(LATENT_CHUNKS):
-        lat_copy(j).wait_send()
+    remote(wo_shard, wo_shard, wox_send, wo_recv.at[0, 0], far_dev).wait_send()
+    remote(lat_own, lat_far, lat_send, lat_recv.at[0], far_dev).wait_send()
     for copy in pair_copies:
         copy.wait_send()
-    for copy in mods:
-        copy.wait_send()
-    line_finish(mod_at, modz_send, modz_recv)
-    line_finish(ctx_at, ctxz_send, ctxz_recv)
+    mods.wait_send()
+    line_finish(lambda count: mod_part.at[0:count], modz_send)
+    line_finish(lambda count: ctx_kv.at[core, 0 : count * ctx_rows], ctxz_send)
     ctx_pair.wait_send()
-    for j in range(sp):
-        for toward, has, sent in ((1, has_right, j <= s), (0, has_left, j >= s)):
-
-            @pl.when(jnp.logical_and(has, sent))
-            def _():
-                def step(c, carry):
-                    wo_line(j, c, toward).wait_send()
-                    return carry
-
-                lax.fori_loop(0, WEIGHT_CHUNKS, step, 0)
-
+    def wo_total(count):
+        return wo.at[far, 0 : count * shard]
+
+    line_finish(wo_total, wo_send)
     wo_sent = wo.at[far, pl.ds(pl.multiple_of(g * sp * shard, 16), sp * shard)]
     remote(wo_sent, wo_sent, woy_send, woy_recv.at[0, 0], y_dev).wait_send()
     wo_pair(0).wait_send()
     wo_pair(1).wait_send()
-    kv_pair(0, t + 1).wait_send()
-    kv_pair(1, far + 1).wait_send()
+    both = key_value.at[:, 0 : 2 * rows]
+    remote(both, both, kv_send, kv_recv.at[0], pair_dev).wait_send()
 
     @pl.when(sends_down)
     def _():
@@ -950,8 +957,7 @@
     def _():
         halo_up.wait_send()
 
-    att_copy(0).wait_send()
-    att_copy(1).wait_send()
+    remote(att_out, att_out, att_send, att_recv.at[0], far_dev).wait_send()
 
 
 def local(
@@ -1050,29 +1056,29 @@
             pltpu.VMEM((2, 2, 2, 1, 2 * rows), f32),
             pltpu.VMEM((tp, rows, out_width), f32),
             dma((12,)),
-            dma((LATENT_CHUNKS,)),
+            dma,
             dma((LATENT_CHUNKS,)),
             dma((2,)),
             dma((5,)),
             dma((5,)),
-            dma((WEIGHT_CHUNKS,)),
-            dma((2, sp, WEIGHT_CHUNKS)),
+            dma,
+            dma((2,)),
             dma((sp, WEIGHT_CHUNKS)),
             dma,
             dma((sp, WEIGHT_CHUNKS)),
             dma((2,)),
             dma((2,)),
-            dma((2, sp)),
+            dma((2,)),
             dma((sp,)),
-            dma((tp - 1,)),
-            dma((tp - 1,)),
-            dma((2, sp)),
+            dma,
+            dma,
+            dma((2,)),
             dma((sp,)),
             dma((2,)),
+            dma,
             dma((2,)),
             dma((2,)),
-            dma((2,)),
-            dma((2,)),
+            dma,
             dma((2,)),
         ],
         compiler_params=pltpu.CompilerParams(

time: 47.5 us -> 44.6 us (0.939)
  Pallas kernels: 46.4 us -> 43.5 us
    pallas_call x1, Pallas kernels: 46.4 us -> 43.5 us  [local(): pl.pallas_call(functools.partial(fused_kernel, sp), out_shape=pltpu.VMEM(...]
where the time goes in v3:
time: 44.6 us; the launch traced here: 44.5 us
  Pallas kernels  43.5 us (98%)
  local copies, waits for them, and re-layouts  0.97 us (2%)
    pallas_call x1, Pallas kernels, local(): pl.pallas_call(functools.partial(fused_kernel, sp), out_shape=pltpu.VMEM(...  43.5 us
    unnamed x1, local copies, waits for them, and re-layouts  0.97 us

profile of v3, /device:TPU:0, one launch (start us, length us, event | category | flops | bytes accessed | tf_op | source)
XLA Modules:
  0.0 44.5 jit_solution(10288498625577334197)
XLA Ops:
  0.0 43.5 %fused.1 = bf16[128,4096]{1,0:T(8,128)(2,1)S(1)} custom-call(bf16[128,4096]{1,0:T(8,128)(2,1)} %latent.1, bf16[192,4096]{1,0:T(8,128)(2,1)} %context.1, bf16[1024]{0:T(1024)(128)(2,1)} %conditioning.1, f32[1,4096]{1,0:T(1,128)} %bitcast.1, bf16[1024,1024]{1,0:T(8,128)(2,1)} %shift_weight.1, bf16[1024,1024]{1,0:T(8,128)(2,1)} %scale_weight.1, ...), custom_call_target="tpu_custom_call" | custom-call | tf_op jit(solution)/shard_map/fused/pallas_call | solution.py:1019
  43.5 1.0 %copy.14 = bf16[128,4096]{1,0:T(8,128)(2,1)} copy(bf16[128,4096]{1,0:T(8,128)(2,1)S(1)} %fused.1) | data formatting | bytes 2097152
